TPU v7x, 32 devices: a whole 2x2x4 slice. The times are simulated.
32 devices in a mesh: sp: 4 (over y, x), tp: 8 (over z, core).
Axes of the slice: x: 2, y: 2, z: 4, core: 2. Of those that a mesh axis runs over, the one named last changes fastest.
Arguments:
- queries: bfloat16 [2048, 1536], P('sp', 'tp'), may hold values from -34 to 34
- latent: bfloat16 [2048, 512], P('sp'), may hold values from -6 to 6
- rot_key: bfloat16 [2048, 32], P('sp'), may hold values from -34 to 34
- latent_gain: float32 [512], replicated, may hold values from 0.1 to 1.9
- key_up: bfloat16 [512, 1024], P(None, 'tp'), may hold values from -0.25 to 0.25
- value_up: bfloat16 [512, 1024], P(None, 'tp'), may hold values from -0.70710678 to 0.70710678
- query_gain: float32 [96], replicated, may hold values from 0.5 to 6
- key_gain: float32 [96], replicated, may hold values from 0.5 to 6
- out_gain: float32 [1024], replicated, may hold values from 0.1 to 1.9
- out_weight: bfloat16 [1024, 2048], replicated, may hold values from -0.1875 to 0.1875
- residual: bfloat16 [2048, 2048], P(('sp', 'tp')), may hold values from -6 to 6
- ffn_gain: float32 [2048], replicated, may hold values from 0.1 to 1.9
- routes: int32 [2048, 2], P(('sp', 'tp')), may hold values from 0 to 3, all different within a row; in each aligned block of 64 rows (0 to 63, 64 to 127, ...) at most 36 rows name the same one
- route_weights: float32 [2048, 2], P(('sp', 'tp')), may hold values from 0.2 to 1
- expert_gate: bfloat16 [4, 2048, 2048], P('sp', None, 'tp'), may hold values from -0.125 to 0.125
- expert_up: bfloat16 [4, 2048, 2048], P('sp', None, 'tp'), may hold values from -0.125 to 0.125
- expert_down: bfloat16 [4, 2048, 2048], P('sp', 'tp'), may hold values from -0.125 to 0.125
Outputs:
- layer_out: bfloat16 [2048, 2048], P(('sp', 'tp'))
Inputs may be any that keep to these rules, and one draw needn't show every extreme that they name: `routes`: the 2 experts of a token differ. Among the 64 rows of one device each expert is named by at most 36 rows, a bound that some block reaches.
All inputs are finite; a program needn't handle non-finite values.
Results may differ from a plain program's by a relative error of at most 0.02.
The roundings to bfloat16 on the way count: a program that leaves them out, or rounds other values in their place, can miss the bound.
Values may be sent and summed in bfloat16 or wider, within the bound.
A program may use at most 128 MiB of HBM per device.

v0:
```python
import functools

import jax
import jax.numpy as jnp
from jax import lax
from jax.experimental import pallas as pl
from jax.experimental.pallas import tpu as pltpu
from jax.sharding import PartitionSpec as P

D = 2048
NOPE = 64
ROPE = 32
VH = 64
TOPK = 2
QK = 96

epsilon = 1e-06
rope_base = 10000.0
MESH_ID = pl.DeviceIdType.MESH


class Place:
    def __init__(self, n_sp, n_z):
        self.n_sp, self.n_z = n_sp, n_z
        self.sp = lax.axis_index("sp")
        self.tp = lax.axis_index("tp")
        self.core = lax.rem(self.tp, 2)
        self.z = lax.div(self.tp, 2)

    def partner(self):
        return (self.sp, self.tp + 1 - 2 * self.core)

    def sp_peer(self, step):
        return lax.rem(self.sp + step, self.n_sp)

    def z_peer(self, step):
        return lax.rem(self.z + step, self.n_z)

    def sp_id(self, index):
        return (index, self.tp)

    def z_id(self, index):
        return (self.sp, 2 * index + self.core)

    def barrier(self, use_sp, use_z):
        sem = pltpu.get_barrier_semaphore()
        count = 1
        pl.semaphore_signal(sem, inc=1, device_id=self.partner(), device_id_type=MESH_ID)
        if use_sp:
            for step in range(1, self.n_sp):
                pl.semaphore_signal(
                    sem, inc=1, device_id=self.sp_id(self.sp_peer(step)), device_id_type=MESH_ID
                )
            count += self.n_sp - 1
        if use_z:
            for step in range(1, self.n_z):
                pl.semaphore_signal(
                    sem, inc=1, device_id=self.z_id(self.z_peer(step)), device_id_type=MESH_ID
                )
            count += self.n_z - 1
        pl.semaphore_wait(sem, count)


def remote(src, dst, send, recv, device):
    return pltpu.make_async_remote_copy(
        src_ref=src,
        dst_ref=dst,
        send_sem=send,
        recv_sem=recv,
        device_id=device,
        device_id_type=MESH_ID,
    )


def vmem():
    return pl.BlockSpec(memory_space=pltpu.VMEM)


def gather_heads(x, n_sp, n_z):
    n_tp = 2 * n_z

    def kernel(x_ref, o_ref, local_sem, send_sem, recv_sem):
        place = Place(n_sp, n_z)
        sem = pltpu.get_barrier_semaphore()
        for step in range(1, n_tp):
            pl.semaphore_signal(
                sem,
                inc=1,
                device_id=(place.sp, lax.rem(place.tp + step, n_tp)),
                device_id_type=MESH_ID,
            )
        pl.semaphore_wait(sem, n_tp - 1)
        copies = []
        for step in range(1, n_tp):
            dst = lax.rem(place.tp + step, n_tp)
            copy = remote(
                x_ref.at[lax.rem(dst, 2)],
                o_ref.at[place.tp],
                send_sem.at[step],
                recv_sem.at[step],
                (place.sp, dst),
            )
            copy.start()
            copies.append(copy)
        local = pltpu.make_async_copy(x_ref.at[place.core], o_ref.at[place.tp], local_sem.at[0])
        local.start()
        for copy in copies:
            copy.wait()
        local.wait()

    return pl.pallas_call(
        kernel,
        out_shape=jax.ShapeDtypeStruct((n_tp,) + x.shape[1:], x.dtype),
        in_specs=[vmem()],
        out_specs=vmem(),
        scratch_shapes=[
            pltpu.SemaphoreType.DMA((1,)),
            pltpu.SemaphoreType.DMA((n_tp,)),
            pltpu.SemaphoreType.DMA((n_tp,)),
        ],
        compiler_params=pltpu.CompilerParams(
            collective_id=1, has_side_effects=True, vmem_limit_bytes=60 << 20
        ),
        name="gather_heads",
    )(x)


def first_exchange(bundle, residual, meta, n_sp, n_z):
    def kernel(kv_ref, res_ref, meta_ref, kv_out, res_out, meta_out, local_sem, *sems):
        place = Place(n_sp, n_z)
        place.barrier(True, True)
        moves = (
            (meta_ref, meta_out, n_z, place.z, place.z_peer, place.z_id),
            (res_ref, res_out, n_z, place.z, place.z_peer, place.z_id),
            (kv_ref, kv_out, n_sp, place.sp, place.sp_peer, place.sp_id),
        )
        copies = []
        for number, (src, out, count, me, peer, to_id) in enumerate(moves):
            for step in range(1, count):
                copy = remote(
                    src,
                    out.at[me],
                    sems[2 * number].at[step],
                    sems[2 * number + 1].at[step],
                    to_id(peer(step)),
                )
                copy.start()
                copies.append(copy)
            local = pltpu.make_async_copy(src, out.at[me], local_sem.at[number])
            local.start()
            copies.append(local)
        for copy in copies:
            copy.wait()

    dma = pltpu.SemaphoreType.DMA
    return pl.pallas_call(
        kernel,
        out_shape=(
            jax.ShapeDtypeStruct((n_sp,) + bundle.shape, bundle.dtype),
            jax.ShapeDtypeStruct((n_z,) + residual.shape, residual.dtype),
            jax.ShapeDtypeStruct((n_z,) + meta.shape, meta.dtype),
        ),
        in_specs=[vmem()] * 3,
        out_specs=(vmem(),) * 3,
        scratch_shapes=[dma((3,))] + [dma((n_z,))] * 4 + [dma((n_sp,))] * 2,
        compiler_params=pltpu.CompilerParams(
            collective_id=0, has_side_effects=True, vmem_limit_bytes=60 << 20
        ),
        name="first_exchange",
    )(bundle, residual, meta)


def send_rows(x, n_sp, n_z):
    rows, shared = x.shape[1], D // 4
    half = (D - shared) // 2

    def kernel(x_ref, o_ref, local_sem, *sems):
        place = Place(n_sp, n_z)
        core, me = place.core, place.sp
        place.barrier(True, True)
        side = lax.rem(place.z, 2)
        twin = place.z_id(place.z + 1 - 2 * side)
        mine = pl.ds(pl.multiple_of(shared + side * half, 128), half)
        other = pl.ds(pl.multiple_of(shared + (1 - side) * half, 128), half)
        both = pl.ds(0, shared)
        copies = []

        def push(kind, step, src, dst, device):
            copy = remote(src, dst, sems[2 * kind].at[step], sems[2 * kind + 1].at[step], device)
            copy.start()
            copies.append(copy)
            return copy

        split, direct, swapped = {}, {}, {}
        for step in range(1, n_sp):
            dst = place.sp_peer(step)
            split[step] = push(
                0, step, x_ref.at[dst, :, mine], o_ref.at[core, me, :, mine], place.sp_id(dst)
            )
        for step in range(1, n_sp):
            dst = place.sp_peer(step)
            direct[step] = push(
                1, step, x_ref.at[dst, :, both], o_ref.at[core, me, :, both], place.sp_id(dst)
            )
        local = pltpu.make_async_copy(x_ref.at[me], o_ref.at[core, me], local_sem.at[0])
        local.start()
        last = [push(3, 0, x_ref.at[me], o_ref.at[core, me], place.partner())]
        for step in range(1, n_sp):
            src = lax.rem(me - step + n_sp, n_sp)
            piece = o_ref.at[core, src, :, mine]
            split[step].wait_recv()
            swapped[step] = push(2, step, piece, piece, twin)
            last.append(push(3, step, piece, piece, place.partner()))
        for step in range(1, n_sp):
            src = lax.rem(me - step + n_sp, n_sp)
            piece = o_ref.at[core, src, :, both]
            direct[step].wait_recv()
            last.append(push(4, step, piece, piece, place.partner()))
        for step in range(1, n_sp):
            src = lax.rem(me - step + n_sp, n_sp)
            piece = o_ref.at[core, src, :, other]
            swapped[step].wait_recv()
            last.append(push(5, step, piece, piece, place.partner()))
        for copy in last:
            copy.wait_recv()
        for copy in copies:
            copy.wait_send()
        local.wait()

    return pl.pallas_call(
        kernel,
        out_shape=jax.ShapeDtypeStruct((2, n_sp, rows, D), x.dtype),
        in_specs=[vmem()],
        out_specs=vmem(),
        scratch_shapes=[pltpu.SemaphoreType.DMA((1,))] + [pltpu.SemaphoreType.DMA((n_sp,))] * 12,
        compiler_params=pltpu.CompilerParams(
            collective_id=2, has_side_effects=True, vmem_limit_bytes=60 << 20
        ),
        name="send_rows",
    )(x)


CHUNKS = 4


def return_rows(hidden, down, mixer, middle, n_sp, n_z):
    rows = hidden.shape[2]
    tok = middle.shape[0]
    width = D // CHUNKS

    def kernel(h_ref, w_ref, mix_ref, mid_ref, o_ref, ybuf, pbuf, sbuf, rbuf, cbuf, fbuf, *sems):
        pair_s, pair_r, sp_s, sp_r, z_s, z_r = sems
        place = Place(n_sp, n_z)
        core = place.core
        place.barrier(True, True)
        pairs, sends, zsends = {}, {}, {}
        order = list(range(1, n_sp)) + [0]
        for q in range(CHUNKS):
            cols = pl.ds(q * width, width)
            for step in order:
                dst = place.sp_peer(step)
                ybuf[dst, :, cols] = jnp.dot(
                    h_ref[1 - core, dst], w_ref[:, cols], preferred_element_type=jnp.float32
                ).astype(jnp.bfloat16)
                copy = remote(
                    ybuf.at[dst, :, cols],
                    pbuf.at[dst, :, cols],
                    pair_s.at[q, step],
                    pair_r.at[q, step],
                    place.partner(),
                )
                copy.start()
                pairs[q, step] = copy
        for q in range(CHUNKS):
            cols = pl.ds(q * width, width)
            for step in order:
                dst = place.sp_peer(step)
                own = jnp.dot(
                    h_ref[core, dst], w_ref[:, cols], preferred_element_type=jnp.float32
                )
                pairs[q, step].wait_recv()
                total = (own + pbuf[dst, :, cols].astype(jnp.float32)).astype(jnp.bfloat16)
                if step == 0:
                    rbuf[dst, :, cols] = total
                else:
                    sbuf[dst, :, cols] = total
                    copy = remote(
                        sbuf.at[dst, :, cols],
                        rbuf.at[place.sp, :, cols],
                        sp_s.at[q, step],
                        sp_r.at[q, step],
                        place.sp_id(dst),
                    )
                    copy.start()
                    sends[q, step] = copy
        for q in range(CHUNKS):
            cols = pl.ds(q * width, width)
            for step in range(1, n_sp):
                sends[q, step].wait_recv()
            combined = jnp.zeros((n_z * tok, width), jnp.float32)
            for src in range(n_sp):
                combined += jnp.dot(
                    mix_ref[src], rbuf[src, :, cols], preferred_element_type=jnp.float32
                )
            cbuf[:, :, cols] = combined.astype(jnp.bfloat16).reshape(n_z, tok, width)
            for step in range(1, n_z):
                dst = place.z_peer(step)
                copy = remote(
                    cbuf.at[dst, :, cols],
                    fbuf.at[place.z, :, cols],
                    z_s.at[q, step],
                    z_r.at[q, step],
                    place.z_id(dst),
                )
                copy.start()
                zsends[q, step] = copy
        for q in range(CHUNKS):
            cols = pl.ds(q * width, width)
            total = mid_ref[:, cols] + cbuf[place.z, :, cols].astype(jnp.float32)
            for step in range(1, n_z):
                src = lax.rem(place.z - step + n_z, n_z)
                zsends[q, step].wait_recv()
                total += fbuf[src, :, cols].astype(jnp.float32)
            o_ref[:, cols] = total.astype(jnp.bfloat16)
        for group in (pairs, sends, zsends):
            for copy in group.values():
                copy.wait_send()

    dma = pltpu.SemaphoreType.DMA
    block = pltpu.VMEM((n_sp, rows, D), jnp.bfloat16)
    zblock = pltpu.VMEM((n_z, tok, D), jnp.bfloat16)
    return pl.pallas_call(
        kernel,
        out_shape=jax.ShapeDtypeStruct((tok, D), jnp.bfloat16),
        in_specs=[vmem()] * 4,
        out_specs=vmem(),
        scratch_shapes=[block, block, block, block, zblock, zblock]
        + [dma((CHUNKS, n_sp))] * 4
        + [dma((CHUNKS, n_z))] * 2,
        compiler_params=pltpu.CompilerParams(
            collective_id=3, has_side_effects=True, vmem_limit_bytes=60 << 20
        ),
        name="return_rows",
    )(hidden, down, mixer, middle)


def rms_scale(values):
    return lax.rsqrt(jnp.mean(values * values, axis=-1, keepdims=True) + epsilon)


def rotate_half(values, angles):
    half_dims = values.shape[-1] // 2
    first_half = values[..., :half_dims]
    second_half = values[..., half_dims:]
    cosine = jnp.cos(angles)
    sine_val = jnp.sin(angles)
    return jnp.concatenate(
        [
            first_half * cosine - second_half * sine_val,
            second_half * cosine + first_half * sine_val,
        ],
        axis=-1,
    )


def head_prepare(raw_rows, gain_vec, angles):
    normed_rows = raw_rows * rms_scale(raw_rows) * gain_vec
    turned_rows = rotate_half(normed_rows[..., NOPE:], angles[:, None, :])
    return jnp.concatenate([normed_rows[..., :NOPE], turned_rows], axis=-1).astype(jnp.bfloat16)


def shards(
    queries,
    latent,
    rot_key,
    latent_gain,
    key_up,
    value_up,
    query_gain,
    key_gain,
    out_gain,
    out_weight,
    residual,
    ffn_gain,
    routes,
    route_weights,
    expert_gate,
    expert_up,
    expert_down,
):
    shard_len = queries.shape[0]
    local_heads = key_up.shape[1] // NOPE
    sp_count = lax.axis_size("sp")
    tp_count = lax.axis_size("tp")
    z_count = tp_count // 2
    tok_count = residual.shape[0]
    my_first = lax.axis_index("sp") * shard_len
    my_last = my_first + shard_len - 1
    positions = my_first + jnp.arange(shard_len, dtype=jnp.int32)
    inverse = rope_base ** (-jnp.arange(0, ROPE, 2, dtype=jnp.float32) / ROPE)
    angles = positions.astype(jnp.float32)[:, None] * inverse[None, :]
    lat_f32 = latent.astype(jnp.float32)
    normed_latent = (lat_f32 * rms_scale(lat_f32) * latent_gain).astype(jnp.bfloat16)
    key_nope = jnp.dot(normed_latent, key_up, preferred_element_type=jnp.float32).astype(
        jnp.bfloat16
    )
    value_rows = jnp.dot(normed_latent, value_up, preferred_element_type=jnp.float32).astype(
        jnp.bfloat16
    )
    shared = jnp.broadcast_to(
        rot_key.astype(jnp.float32)[:, None, :], (shard_len, local_heads, ROPE)
    )
    raw_keys = jnp.concatenate(
        [key_nope.astype(jnp.float32).reshape(shard_len, local_heads, NOPE), shared], axis=-1
    )
    key_rows = head_prepare(raw_keys, key_gain, angles)
    query_rows = head_prepare(
        queries.astype(jnp.float32).reshape(shard_len, local_heads, QK), query_gain, angles
    )
    query_heads = jnp.transpose(query_rows, (1, 0, 2))
    bundle = jnp.concatenate(
        [
            jnp.transpose(key_rows, (1, 2, 0)),
            jnp.transpose(value_rows.reshape(shard_len, local_heads, VH), (1, 2, 0)),
        ],
        axis=1,
    )
    score_scale = QK ** (-0.5)
    init_state = (
        jnp.full((local_heads, shard_len), -1e30, jnp.float32),
        jnp.zeros((local_heads, shard_len), jnp.float32),
        jnp.zeros((local_heads, shard_len, VH), jnp.float32),
    )
    meta = jnp.concatenate(
        [
            routes.astype(jnp.float32),
            route_weights,
            jnp.zeros((tok_count, 128 - 2 * TOPK), jnp.float32),
        ],
        axis=1,
    )
    key_piece, residual_all, meta_all = first_exchange(bundle, residual, meta, sp_count, z_count)
    block_count = sp_count

    def one_block(block_index, running_state):
        first_key = block_index * shard_len

        def compute(inner):
            row_peak, row_total, weighted = inner
            key_part = lax.dynamic_index_in_dim(key_piece, block_index, 0, keepdims=False)
            scores = (
                jnp.einsum(
                    "hqc,hck->hqk",
                    query_heads,
                    key_part[:, :QK, :],
                    preferred_element_type=jnp.float32,
                )
                * score_scale
            )
            key_pos = first_key + jnp.arange(shard_len, dtype=jnp.int32)
            allowed = key_pos[None, None, :] <= positions[None, :, None]
            scores = jnp.where(allowed, scores, -1e30)
            new_peak = jnp.maximum(row_peak, jnp.max(scores, axis=2))
            exponent = jnp.where(allowed, jnp.exp(scores - new_peak[..., None]), 0.0)
            factor = jnp.exp(row_peak - new_peak)
            new_total = row_total * factor + jnp.sum(exponent, axis=2)
            contrib = jnp.einsum(
                "hqk,hvk->hqv",
                exponent.astype(jnp.bfloat16),
                key_part[:, QK:, :],
                preferred_element_type=jnp.float32,
            )
            return (new_peak, new_total, weighted * factor[..., None] + contrib)

        return lax.cond(first_key <= my_last, compute, lambda inner: inner, running_state)

    row_peak, row_total, weighted = lax.fori_loop(0, block_count, one_block, init_state)
    attended = (weighted / row_total[..., None]).astype(jnp.bfloat16)
    part_len = z_count * tok_count
    by_core = (
        attended.reshape(local_heads, z_count, 2, tok_count, VH)
        .transpose(2, 1, 3, 0, 4)
        .reshape(2, part_len, local_heads * VH)
    )
    gathered = gather_heads(by_core, sp_count, z_count)
    att_rows = jnp.transpose(gathered, (1, 0, 2)).reshape(part_len, -1).astype(jnp.float32)
    normed_rows = (att_rows * rms_scale(att_rows) * out_gain).astype(jnp.bfloat16)
    mixed = jnp.dot(normed_rows, out_weight, preferred_element_type=jnp.float32)
    middle = residual_all.reshape(part_len, D).astype(jnp.float32) + mixed
    part_input = (middle * rms_scale(middle) * ffn_gain).astype(jnp.bfloat16)
    own_middle = lax.dynamic_slice_in_dim(
        middle, lax.axis_index("tp") // 2 * tok_count, tok_count, 0
    )
    slot_cap = max(2, 9 * tok_count * TOPK // (8 * sp_count))
    rows = z_count * slot_cap
    part_routes = meta_all[:, :, :TOPK].astype(jnp.int32).reshape(z_count, tok_count * TOPK)
    part_weights = meta_all[:, :, TOPK : 2 * TOPK].reshape(z_count * tok_count, TOPK)
    one_hot = (part_routes[:, :, None] == jnp.arange(sp_count, dtype=jnp.int32)).astype(jnp.int32)
    earlier = jnp.cumsum(one_hot, axis=1) - one_hot
    rank_in = jnp.sum(earlier * one_hot, axis=2)
    slots = rank_in + jnp.arange(z_count, dtype=jnp.int32)[:, None] * slot_cap
    targets = (part_routes * rows + slots).reshape(z_count * tok_count, TOPK)
    hits = targets[:, :, None] == jnp.arange(sp_count * rows, dtype=jnp.int32)
    chooser = jnp.sum(hits.astype(jnp.bfloat16), axis=1)
    mixer = jnp.sum(jnp.where(hits, part_weights[:, :, None], 0.0), axis=1).astype(jnp.bfloat16)
    mixer = jnp.transpose(mixer.reshape(z_count * tok_count, sp_count, rows), (1, 0, 2))
    outbound = (
        jnp.einsum("ts,td->sd", chooser, part_input, preferred_element_type=jnp.float32)
        .astype(jnp.bfloat16)
        .reshape(sp_count, rows, D)
    )
    arrived = send_rows(outbound, sp_count, z_count)
    row_block = arrived.reshape(2 * sp_count * rows, D)
    gate_pre = jnp.dot(row_block, expert_gate[0], preferred_element_type=jnp.float32)
    up_pre = jnp.dot(row_block, expert_up[0], preferred_element_type=jnp.float32)
    hidden = (jax.nn.silu(gate_pre) * up_pre).astype(jnp.bfloat16)
    return return_rows(
        hidden.reshape(2, sp_count, rows, -1),
        expert_down[0],
        mixer,
        own_middle,
        sp_count,
        z_count,
    )


def solution(mesh):
    return jax.shard_map(
        shards,
        mesh=mesh,
        in_specs=(
            P("sp", "tp"),
            P("sp", None),
            P("sp", None),
            P(),
            P(None, "tp"),
            P(None, "tp"),
            P(),
            P(),
            P(),
            P(),
            P(("sp", "tp"), None),
            P(),
            P(("sp", "tp"), None),
            P(("sp", "tp"), None),
            P("sp", None, "tp"),
            P("sp", None, "tp"),
            P("sp", "tp", None),
        ),
        out_specs=P(("sp", "tp"), None),
        check_vma=False,
    )
```

profile of v0, /device:TPU:0, one launch (start us, length us, event | category | flops | bytes accessed | tf_op | source)
XLA Modules:
  0.0 166.4 jit_solution(6021606868210834373)
XLA Ops:
  0.1 0.8 convert_element_type.97
  1.1 1.2 fusion.18
  2.3 1.0 fusion.30
  3.5 0.8 copy.32
  4.3 0.7 maximum_maximum_fusion.meta_ref
  5.2 0.8 broadcast_in_dim.42
  5.9 1.5 convolution_convert_fusion.1
  7.5 0.4 bitcast_convert_fusion
  8.3 0.8 pad_maximum_fusion.1.kv_ref
  9.1 30.1 %first_exchange.1 = (bf16[4,2,160,512]{3,2,1,0:T(8,128)(2,1)S(1)}, bf16[4,64,2048]{2,1,0:T(8,128)(2,1)}, f32[4,64,128]{2,1,0:T(8,128)}) custom-call(bf16[2,160,512]{2,1,0:T(8,128)(2,1)} %pad_maximum_fusion.1.kv_ref, bf16[64,2048]{1,0:T(8,128)(2,1)} %res_ref.1, f32[64,128]{1,0:T(8,128)} %maximum_maximum_fusion.meta_ref), custom_call_target="tpu_custom_call" | custom-call | tf_op jit(solution)/shard_map/first_exchange/pallas_call | solution.py:156
  39.2 2.6 %while.18 = (s32[]{:T(128)}, f32[2,512]{1,0:T(2,128)S(1)}, f32[2,512]{1,0:T(2,128)S(1)}, f32[2,512,64]{1,2,0:T(8,128)S(1)}, s32[]{:T(128)}, /*index=5*/bf16[4,2,...) while((s32[]{:T(128)}, f32[2,512]{1,0:T(2,128)S(1)}, ...), condition=%wide.region_11.12_spmd.clone, body=%wide.region_6.11_spmd.clone.sunk | while | flops 174984192 | bytes 9122101 | solution.py:477
  39.3 2.3 %conditional.3 = ((f32[2,512]{1,0:T(2,128)S(1)}, f32[2,512]{1,0:T(2,128)S(1)}, f32[2,512,64]{1,2,0:T(8,128)S(1)})) conditional(s32[]{:T(128)} %convert_element_type.160, (f32[2,512]{1,0:T(2,128)S(1)}, f32[2,512]{1,0:T(2,128)S(1)}, f32[2,512,64]{1,2,0:T(8,128)S(1)}) %tuple.53, (s32[]{:T(128)}, s32[]{:T(128)}, s32[]{:T(128)}, ...), branch_computations={%region_7.7_spmd, %region_8.10_spmd} | conditional | flops 174984192 | bytes 9119822 | solution.py:475
  39.6 0.6 fusion.2
  40.2 0.6 fusion.4
  40.8 0.8 convolution_add_fusion
  42.0 0.4 copy.36
  42.4 0.8 reshape.223.x_ref
  43.4 0.5 copy.33
  45.3 1.0 copy.39
  46.5 17.1 %gather_heads.1 = bf16[8,256,128]{2,1,0:T(8,128)(2,1)} custom-call(bf16[2,256,128]{2,1,0:T(8,128)(2,1)} %reshape.223.x_ref), custom_call_target="tpu_custom_call" | custom-call | tf_op jit(solution)/shard_map/gather_heads/pallas_call | solution.py:111
  63.6 1.2 fusion.21
  64.8 1.1 convert_bitcast_fusion
  65.9 0.3 copy.37
  66.5 1.0 copy-done.3
  67.5 3.6 %multiply_reduce_fusion = (f32[256]{0:T(256)S(1)}, f32[256,2048]{1,0:T(8,128)S(1)}) fusion(bf16[256,1024]{0,1:T(8,128)(2,1)S(1)} %fusion.26, bf16[1024,2048]{1,0:T(8,128)(2,1)} %param.30, bf16[256,2048]{1,0:T(8,128)(2,1)S(1)} %bitcast.68), kind=kOutput, calls=%fused_computation.28 | convolution fusion | flops 1075838720 | bytes 7865344 | tf_op jit(solution)/shard_map/dot_general | solution.py:488
  71.1 0.8 constant_dynamic-slice_fusion.mid_ref
  72.0 2.4 %convolution_convert_fusion = bf16[576,2048]{1,0:T(8,128)(2,1)} fusion(bf16[256,576]{0,1:T(8,128)(2,1)S(1)} %fusion.29, f32[256,2048]{1,0:T(8,128)S(1)} %get-tuple-element.250, f32[2048]{0:T(1024)S(1)} %copy-done.6, f32[256]{0:T(256)S(1)} %add_rsqrt_fusion.3), kind=kOutput, calls=%fused_computation.23 | convolution fusion | flops 606732288 | bytes 4760576 | tf_op jit(solution)/shard_map/ts,td->sd/dot_general | solution.py:508
  74.3 41.3 %send_rows.1 = bf16[2,4,144,2048]{3,2,1,0:T(8,128)(2,1)} custom-call(bf16[4,144,2048]{2,1,0:T(8,128)(2,1)} %bitcast.62), custom_call_target="tpu_custom_call" | custom-call | tf_op jit(solution)/shard_map/send_rows/pallas_call | solution.py:230
  115.7 3.9 %fusion.23 = f32[1152,256]{1,0:T(8,128)S(1)} fusion(bf16[1152,2048]{1,0:T(8,128)(2,1)} %bitcast.63, bf16[1,2048,256]{2,1,0:T(8,128)(2,1)S(1)} %copy-done), kind=kOutput, calls=%fused_computation.43 | convolution fusion | flops 1207959552 | bytes 6946816 | tf_op jit(solution)/shard_map/dot_general | solution.py:514
  119.8 2.3 %fusion.16 = bf16[1152,256]{1,0:T(8,128)(2,1)} fusion(bf16[1152,2048]{1,0:T(8,128)(2,1)S(1)} %bitcast.64, f32[1152,256]{1,0:T(8,128)S(1)} %fusion.23, bf16[1,2048,256]{2,1,0:T(8,128)(2,1)S(1)} %copy-done.10), kind=kOutput, calls=%fused_computation.26 | convolution fusion | flops 1209729024 | bytes 7536640 | tf_op jit(solution)/shard_map/dot_general | solution.py:515
  122.1 42.7 %return_rows.1 = bf16[64,2048]{1,0:T(8,128)(2,1)} custom-call(bf16[2,4,144,256]{3,2,1,0:T(8,128)(2,1)} %bitcast.72, bf16[256,2048]{1,0:T(8,128)(2,1)} %bitcast.67, bf16[4,256,144]{2,1,0:T(8,128)(2,1)} %bitcast.65, f32[64,2048]{1,0:T(8,128)} %constant_dynamic-slice_fusion.mid_ref), custom_call_target="tpu_custom_call" | custom-call | tf_op jit(solution)/shard_map/return_rows/pallas_call | solution.py:332
  164.8 1.7 %copy.60 = bf16[64,2048]{1,0:T(8,128)(2,1)} copy(bf16[64,2048]{1,0:T(8,128)(2,1)} %return_rows.1) | data formatting | bytes 524288
  (77 shorter events, 3.6 us)
Async XLA Ops:
  0.0 115.7 %copy-start = (bf16[1,2048,256]{2,1,0:T(8,128)(2,1)S(1)}, bf16[1,2048,256]{2,1,0:T(8,128)(2,1)}, u32[]{:S(2)}) copy-start(bf16[1,2048,256]{2,1,0:T(8,128)(2,1)} %param.35) | copy-start | bytes 3145732
  0.0 7.5 %copy-start.5 = (bf16[512,512]{1,0:T(8,128)(2,1)S(1)}, bf16[512,512]{1,0:T(8,128)(2,1)}, u32[]{:S(2)}) copy-start(bf16[512,512]{1,0:T(8,128)(2,1)} %param.22) | copy-start | bytes 1572868
  0.0 7.5 %copy-start.12 = (f32[512]{0:T(512)S(1)}, f32[512]{0:T(512)}, u32[]{:S(2)}) copy-start(f32[512]{0:T(512)} %param.24) | copy-start | bytes 6148
  0.0 8.0 %copy-start.8 = (f32[96]{0:T(128)S(1)}, f32[96]{0:T(128)}, u32[]{:S(2)}) copy-start(f32[96]{0:T(128)} %param.28) | copy-start | bytes 1156
  0.0 7.5 %copy-start.11 = (bf16[512,128]{1,0:T(8,128)(2,1)S(1)}, bf16[512,128]{1,0:T(8,128)(2,1)}, u32[]{:S(2)}) copy-start(bf16[512,128]{1,0:T(8,128)(2,1)} %param.25) | copy-start | bytes 393220
  2.3 5.8 %copy-start.4 = (bf16[512,192]{0,1:T(8,128)(2,1)S(1)}, bf16[512,192]{0,1:T(8,128)(2,1)}, u32[]{:S(2)}) copy-start(bf16[512,192]{0,1:T(8,128)(2,1)} %param.21) | copy-start | bytes 589828
  2.3 5.8 %copy-start.9 = (f32[96]{0:T(128)S(1)}, f32[96]{0:T(128)}, u32[]{:S(2)}) copy-start(f32[96]{0:T(128)} %param.27) | copy-start | bytes 1156
  39.2 4.0 %copy-start.2 = (f32[4,64,128]{2,1,0:T(8,128)S(1)}, f32[4,64,128]{2,1,0:T(8,128)}, u32[]{:S(2)}) copy-start(f32[4,64,128]{2,1,0:T(8,128)} %get-tuple-element.187) | copy-start | bytes 393220
  63.6 2.7 %copy-start.7 = (f32[1024]{0:T(1024)S(1)}, f32[1024]{0:T(1024)}, u32[]{:S(2)}) copy-start(f32[1024]{0:T(1024)} %param.29) | copy-start | bytes 12292
  66.3 1.2 copy-start.3
  67.5 4.4 %copy-start.6 = (f32[2048]{0:T(1024)S(1)}, f32[2048]{0:T(1024)}, u32[]{:S(2)}) copy-start(f32[2048]{0:T(1024)} %param.32) | copy-start | bytes 24580
  115.7 3.9 %copy-start.1 = (bf16[2,4,144,2048]{3,2,1,0:T(8,128)(2,1)S(1)}, bf16[2,4,144,2048]{3,2,1,0:T(8,128)(2,1)}, u32[]{:S(2)}) copy-start(bf16[2,4,144,2048]{3,2,1,0:T(8,128)(2,1)} %send_rows.1) | copy-start | bytes 14155780
  115.7 4.1 %copy-start.10 = (bf16[1,2048,256]{2,1,0:T(8,128)(2,1)S(1)}, bf16[1,2048,256]{2,1,0:T(8,128)(2,1)}, u32[]{:S(2)}) copy-start(bf16[1,2048,256]{2,1,0:T(8,128)(2,1)} %param.36) | copy-start | bytes 3145732
where the time goes:
time: 167 us; the launch traced here: 166 us
  Pallas kernels  131 us (78%)
  matrix products  15.5 us (9%)
  other arithmetic  9.79 us (6%)
  local copies, waits for them, and re-layouts  9.3 us (6%)
    pallas_call x1, Pallas kernels, return_rows(): pl.pallas_call(kernel, out_shape=jax.ShapeDtypeStruct((tok, D), jnp.bfloa...  42.7 us
    pallas_call x1, Pallas kernels, send_rows(): pl.pallas_call(kernel, out_shape=jax.ShapeDtypeStruct((2, n_sp, rows, D),...  41.3 us
    pallas_call x1, Pallas kernels, first_exchange(): pl.pallas_call(kernel, out_shape=(jax.ShapeDtypeStruct((n_sp,) + bundle.s...  30.1 us
    pallas_call x1, Pallas kernels, gather_heads(): pl.pallas_call(kernel, out_shape=jax.ShapeDtypeStruct((n_tp,) + x.shape[1...  17.1 us
    dot_general x1, matrix products, shards(): jnp.dot(row_block, expert_gate[0], preferred_element_type=jnp.float32)  3.89 us
    unnamed x28, local copies, waits for them, and re-layouts  3.64 us
    dot_general x1, matrix products, shards(): mixed = jnp.dot(normed_rows, out_weight, preferred_element_type=jnp.float32)  3.58 us
    reduce_sum x4, other arithmetic, rms_scale(): jnp.mean(values * values, axis=-1, keepdims=True) + epsilon  3.54 us

commit v1 on v0

v1 whole, which is shorter than its diff:
```python
import jax
import jax.numpy as jnp
from jax import lax
from jax.experimental import pallas as pl
from jax.experimental.pallas import tpu as pltpu
from jax.sharding import PartitionSpec as P

D = 2048
NOPE = 64
ROPE = 32
VH = 64
TOPK = 2
QK = 96

epsilon = 1e-06
rope_base = 10000.0
MESH_ID = pl.DeviceIdType.MESH


class Place:
    def __init__(self, n_sp, n_z):
        self.n_sp, self.n_z = n_sp, n_z
        self.sp = lax.axis_index("sp")
        self.tp = lax.axis_index("tp")
        self.core = lax.rem(self.tp, 2)
        self.z = lax.div(self.tp, 2)

    def partner(self):
        return (self.sp, self.tp + 1 - 2 * self.core)

    def sp_peer(self, step):
        return lax.rem(self.sp + step, self.n_sp)

    def z_peer(self, step):
        return lax.rem(self.z + step, self.n_z)

    def sp_id(self, index):
        return (index, self.tp)

    def z_id(self, index):
        return (self.sp, 2 * index + self.core)

    def barrier(self, use_sp, use_z):
        sem = pltpu.get_barrier_semaphore()
        count = 1
        pl.semaphore_signal(sem, inc=1, device_id=self.partner(), device_id_type=MESH_ID)
        if use_sp:
            for step in range(1, self.n_sp):
                pl.semaphore_signal(
                    sem, inc=1, device_id=self.sp_id(self.sp_peer(step)), device_id_type=MESH_ID
                )
            count += self.n_sp - 1
        if use_z:
            for step in range(1, self.n_z):
                pl.semaphore_signal(
                    sem, inc=1, device_id=self.z_id(self.z_peer(step)), device_id_type=MESH_ID
                )
            count += self.n_z - 1
        pl.semaphore_wait(sem, count)


def remote(src, dst, send, recv, device):
    return pltpu.make_async_remote_copy(
        src_ref=src,
        dst_ref=dst,
        send_sem=send,
        recv_sem=recv,
        device_id=device,
        device_id_type=MESH_ID,
    )


def vmem():
    return pl.BlockSpec(memory_space=pltpu.VMEM)


def send_rows(x, n_sp, n_z):
    rows, shared = x.shape[1], D // 4
    half = (D - shared) // 2

    def kernel(x_ref, o_ref, local_sem, *sems):
        place = Place(n_sp, n_z)
        core, me = place.core, place.sp
        place.barrier(True, True)
        side = lax.rem(place.z, 2)
        twin = place.z_id(place.z + 1 - 2 * side)
        mine = pl.ds(pl.multiple_of(shared + side * half, 128), half)
        other = pl.ds(pl.multiple_of(shared + (1 - side) * half, 128), half)
        both = pl.ds(0, shared)
        copies = []

        def push(kind, step, src, dst, device):
            copy = remote(src, dst, sems[2 * kind].at[step], sems[2 * kind + 1].at[step], device)
            copy.start()
            copies.append(copy)
            return copy

        split, direct, swapped = {}, {}, {}
        for step in range(1, n_sp):
            dst = place.sp_peer(step)
            split[step] = push(
                0, step, x_ref.at[dst, :, mine], o_ref.at[core, me, :, mine], place.sp_id(dst)
            )
        for step in range(1, n_sp):
            dst = place.sp_peer(step)
            direct[step] = push(
                1, step, x_ref.at[dst, :, both], o_ref.at[core, me, :, both], place.sp_id(dst)
            )
        local = pltpu.make_async_copy(x_ref.at[me], o_ref.at[core, me], local_sem.at[0])
        local.start()
        last = [push(3, 0, x_ref.at[me], o_ref.at[core, me], place.partner())]
        for step in range(1, n_sp):
            src = lax.rem(me - step + n_sp, n_sp)
            piece = o_ref.at[core, src, :, mine]
            split[step].wait_recv()
            swapped[step] = push(2, step, piece, piece, twin)
            last.append(push(3, step, piece, piece, place.partner()))
        for step in range(1, n_sp):
            src = lax.rem(me - step + n_sp, n_sp)
            piece = o_ref.at[core, src, :, both]
            direct[step].wait_recv()
            last.append(push(4, step, piece, piece, place.partner()))
        for step in range(1, n_sp):
            src = lax.rem(me - step + n_sp, n_sp)
            piece = o_ref.at[core, src, :, other]
            swapped[step].wait_recv()
            last.append(push(5, step, piece, piece, place.partner()))
        for copy in last:
            copy.wait_recv()
        for copy in copies:
            copy.wait_send()
        local.wait()

    return pl.pallas_call(
        kernel,
        out_shape=jax.ShapeDtypeStruct((2, n_sp, rows, D), x.dtype),
        in_specs=[vmem()],
        out_specs=vmem(),
        scratch_shapes=[pltpu.SemaphoreType.DMA((1,))] + [pltpu.SemaphoreType.DMA((n_sp,))] * 12,
        compiler_params=pltpu.CompilerParams(
            collective_id=2, has_side_effects=True, vmem_limit_bytes=60 << 20
        ),
        name="send_rows",
    )(x)


CHUNKS = 4


def return_rows(hidden, down, mixer, middle, n_sp, n_z):
    rows = hidden.shape[2]
    tok = middle.shape[0]
    width = D // CHUNKS

    def kernel(h_ref, w_ref, mix_ref, mid_ref, o_ref, ybuf, pbuf, sbuf, rbuf, cbuf, fbuf, *sems):
        pair_s, pair_r, sp_s, sp_r, z_s, z_r = sems
        place = Place(n_sp, n_z)
        core = place.core
        place.barrier(True, True)
        pairs, sends, zsends = {}, {}, {}
        order = list(range(1, n_sp)) + [0]
        for q in range(CHUNKS):
            cols = pl.ds(q * width, width)
            for step in order:
                dst = place.sp_peer(step)
                ybuf[dst, :, cols] = jnp.dot(
                    h_ref[1 - core, dst], w_ref[:, cols], preferred_element_type=jnp.float32
                ).astype(jnp.bfloat16)
                copy = remote(
                    ybuf.at[dst, :, cols],
                    pbuf.at[dst, :, cols],
                    pair_s.at[q, step],
                    pair_r.at[q, step],
                    place.partner(),
                )
                copy.start()
                pairs[q, step] = copy
        for q in range(CHUNKS):
            cols = pl.ds(q * width, width)
            for step in order:
                dst = place.sp_peer(step)
                own = jnp.dot(
                    h_ref[core, dst], w_ref[:, cols], preferred_element_type=jnp.float32
                )
                pairs[q, step].wait_recv()
                total = (own + pbuf[dst, :, cols].astype(jnp.float32)).astype(jnp.bfloat16)
                if step == 0:
                    rbuf[dst, :, cols] = total
                else:
                    sbuf[dst, :, cols] = total
                    copy = remote(
                        sbuf.at[dst, :, cols],
                        rbuf.at[place.sp, :, cols],
                        sp_s.at[q, step],
                        sp_r.at[q, step],
                        place.sp_id(dst),
                    )
                    copy.start()
                    sends[q, step] = copy
        for q in range(CHUNKS):
            cols = pl.ds(q * width, width)
            for step in range(1, n_sp):
                sends[q, step].wait_recv()
            combined = jnp.zeros((n_z * tok, width), jnp.float32)
            for src in range(n_sp):
                combined += jnp.dot(
                    mix_ref[src], rbuf[src, :, cols], preferred_element_type=jnp.float32
                )
            cbuf[:, :, cols] = combined.astype(jnp.bfloat16).reshape(n_z, tok, width)
            for step in range(1, n_z):
                dst = place.z_peer(step)
                copy = remote(
                    cbuf.at[dst, :, cols],
                    fbuf.at[place.z, :, cols],
                    z_s.at[q, step],
                    z_r.at[q, step],
                    place.z_id(dst),
                )
                copy.start()
                zsends[q, step] = copy
        for q in range(CHUNKS):
            cols = pl.ds(q * width, width)
            total = mid_ref[:, cols] + cbuf[place.z, :, cols].astype(jnp.float32)
            for step in range(1, n_z):
                src = lax.rem(place.z - step + n_z, n_z)
                zsends[q, step].wait_recv()
                total += fbuf[src, :, cols].astype(jnp.float32)
            o_ref[:, cols] = total.astype(jnp.bfloat16)
        for group in (pairs, sends, zsends):
            for copy in group.values():
                copy.wait_send()

    dma = pltpu.SemaphoreType.DMA
    block = pltpu.VMEM((n_sp, rows, D), jnp.bfloat16)
    zblock = pltpu.VMEM((n_z, tok, D), jnp.bfloat16)
    return pl.pallas_call(
        kernel,
        out_shape=jax.ShapeDtypeStruct((tok, D), jnp.bfloat16),
        in_specs=[vmem()] * 4,
        out_specs=vmem(),
        scratch_shapes=[block, block, block, block, zblock, zblock]
        + [dma((CHUNKS, n_sp))] * 4
        + [dma((CHUNKS, n_z))] * 2,
        compiler_params=pltpu.CompilerParams(
            collective_id=3, has_side_effects=True, vmem_limit_bytes=60 << 20
        ),
        name="return_rows",
    )(hidden, down, mixer, middle)


def split_dot(a, b, dims):
    return lax.dot_general(a, b, (dims, ((), ())), preferred_element_type=jnp.float32)


NT = ((1,), (1,))
NN = ((1,), (0,))
TN = ((0,), (0,))


def front(
    queries, latent, rot_key, lat_gain, key_up, value_up, q_gain, k_gain, out_gain,
    out_weight, residual, ffn_gain, routes, weights, cosine, sine, n_sp, n_z, width,
):
    length = queries.shape[0]
    heads = queries.shape[1] // QK
    n_tp = 2 * n_z
    tok = residual.shape[0]
    part = n_z * tok
    cap = max(2, 9 * tok * TOPK // (8 * n_sp))
    rows = n_z * cap
    bundle = 2 * length + length // 2
    half = length // 2
    lanes = 128
    att_width = width
    qt = 256
    pt = 128

    def kernel(
        q_in, lat_in, rot_in, latg, kup, vup, qg, kg, outg, w_hbm, res_in, ffng, routes_in,
        weights_in, cos_in, sin_in, out_rows, mixer, mid_out,
        qbuf, kv, peak, total, acc, att, gath, normed, wbuf, resbuf, metabuf, mid, ffn,
        w_sem, local_sem, kv_s, kv_r, res_s, res_r, meta_s, meta_r, att_s, att_r,
    ):
        place = Place(n_sp, n_z)
        sp, core, z, tp = place.sp, place.core, place.z, place.tp
        load_w = pltpu.make_async_copy(w_hbm, wbuf, w_sem.at[0])
        load_w.start()
        sem = pltpu.get_barrier_semaphore()
        for step in range(1, n_tp):
            pl.semaphore_signal(
                sem, inc=1, device_id=(sp, lax.rem(tp + step, n_tp)), device_id_type=MESH_ID
            )
        for step in range(1, n_sp):
            pl.semaphore_signal(
                sem, inc=1, device_id=place.sp_id(place.sp_peer(step)), device_id_type=MESH_ID
            )

        lane_id = lax.broadcasted_iota(jnp.int32, (tok, lanes), 1)
        r0, r1 = routes_in[:, 0:1], routes_in[:, 1:2]
        named0, named1 = lane_id == r0, lane_id == r1
        named = jnp.where(named0 | named1, 1.0, 0.0)
        earlier = jnp.where(
            lax.broadcasted_iota(jnp.int32, (tok, tok), 1)
            < lax.broadcasted_iota(jnp.int32, (tok, tok), 0),
            1.0,
            0.0,
        ).astype(jnp.bfloat16)
        rank = split_dot(earlier, named.astype(jnp.bfloat16), NN)
        slot = jnp.where(named0 | named1, rank + (z * cap).astype(jnp.float32), -1.0)
        share = jnp.where(named0, weights_in[:, 0:1], 0.0) + jnp.where(
            named1, weights_in[:, 1:2], 0.0
        )
        metabuf[z] = jnp.where(lane_id < 64, slot, pltpu.roll(share, 64, 1))

        pl.semaphore_wait(sem, n_tp - 1 + n_sp - 1)
        sends = []

        def push(src, dst, send, recv, device):
            copy = remote(src, dst, send, recv, device)
            copy.start()
            return copy

        res_copies, meta_copies = [], []
        for step in range(1, n_z):
            to = place.z_id(place.z_peer(step))
            meta_copies.append(
                push(metabuf.at[z], metabuf.at[z], meta_s.at[step], meta_r.at[step], to)
            )
        for step in range(1, n_z):
            to = place.z_id(place.z_peer(step))
            res_copies.append(push(res_in, resbuf.at[z], res_s.at[step], res_r.at[step], to))
        local = pltpu.make_async_copy(res_in, resbuf.at[z], local_sem.at[0])
        local.start()

        lane = lax.broadcasted_iota(jnp.int32, (1, lanes), 1)
        low = lane % ROPE < ROPE // 2
        mine = kv.at[sp]

        def turn(values, cos, sin):
            return (
                values * cos
                + pltpu.roll(values, lanes - ROPE // 2, 1) * jnp.where(low, -sin, 0.0)
                + pltpu.roll(values, ROPE // 2, 1) * jnp.where(low, 0.0, sin)
            )

        sel = lax.broadcasted_iota(jnp.int32, (ROPE, lanes), 0)
        rot_sel = jnp.where(
            (lax.broadcasted_iota(jnp.int32, (ROPE, lanes), 1) % ROPE == sel)
            & (lax.broadcasted_iota(jnp.int32, (ROPE, lanes), 1) < heads * ROPE),
            1.0,
            0.0,
        ).astype(jnp.bfloat16)
        rot_parts = length // pt

        def make_keys(i, carry):
            at = pl.ds(pl.multiple_of(i * pt, pt), pt)
            lat = lat_in[at, :].astype(jnp.float32)
            scale = lax.rsqrt(jnp.mean(lat * lat, axis=-1, keepdims=True) + epsilon)
            normed_lat = (lat * scale * latg[...]).astype(jnp.bfloat16)
            nope = split_dot(normed_lat, kup[...], NN).astype(jnp.bfloat16).astype(jnp.float32)
            vals = split_dot(normed_lat, vup[...], NN).astype(jnp.bfloat16)
            kv[sp, pl.ds(pl.multiple_of(length + i * pt, pt), pt), :] = vals
            rot = split_dot(rot_in[at, :], rot_sel, NN)
            square, rot_square = nope * nope, rot * rot
            nope_scale, rot_scale = None, None
            for h in range(heads):
                in_nope = (lane >= h * NOPE) & (lane < (h + 1) * NOPE)
                in_rot = (lane >= h * ROPE) & (lane < (h + 1) * ROPE)
                one = lax.rsqrt(
                    jnp.sum(
                        jnp.where(in_nope, square, 0.0) + jnp.where(in_rot, rot_square, 0.0),
                        axis=-1,
                        keepdims=True,
                    )
                    / QK
                    + epsilon
                )
                nope_scale = one if h == 0 else jnp.where(in_nope, one, nope_scale)
                rot_scale = one if h == 0 else jnp.where(in_rot, one, rot_scale)
            kv[sp, at, :] = (nope * nope_scale * kg[0:1, :lanes]).astype(jnp.bfloat16)
            turned = turn(rot * rot_scale * kg[0:1, lanes:], cos_in[at, :], sin_in[at, :])
            return turned

        def make_pair(i, carry):
            first = make_keys(i, carry)
            second = make_keys(i + rot_parts // 2, carry)
            packed = first + pltpu.roll(second, 64, 1)
            kv[sp, pl.ds(pl.multiple_of(2 * length + i * pt, pt), pt), :] = packed.astype(
                jnp.bfloat16
            )
            return carry

        lax.fori_loop(0, rot_parts // 2, make_pair, 0)
        for step in range(1, n_sp):
            dst = sp + n_sp - step

            @pl.when(dst < n_sp)
            def _(dst=dst):
                push(mine, mine, kv_s.at[dst], kv_r.at[sp], place.sp_id(dst))

        wide = 2 * lanes
        src_id = lax.broadcasted_iota(jnp.int32, (heads * QK, wide), 0)
        dst_id = lax.broadcasted_iota(jnp.int32, (heads * QK, wide), 1)
        pickers = []
        for h in range(heads):
            entry = src_id - h * QK
            nope_hit = (entry >= 0) & (entry < NOPE) & (dst_id == h * NOPE + entry)
            rot_hit = (
                (entry >= NOPE) & (entry < QK) & (dst_id == lanes + h * ROPE + entry - NOPE)
            )
            pickers.append(jnp.where(nope_hit | rot_hit, 1.0, 0.0).astype(jnp.bfloat16))

        def make_queries(i, carry):
            at = pl.ds(pl.multiple_of(i * pt, pt), pt)
            raw = q_in[at, :]
            for h in range(heads):
                spread = split_dot(raw, pickers[h], NN)
                scale = lax.rsqrt(
                    jnp.sum(spread * spread, axis=-1, keepdims=True) / QK + epsilon
                )
                spread = spread * scale * qg[0:1, :]
                nope = spread[:, :lanes].astype(jnp.bfloat16)
                rot = turn(spread[:, lanes:], cos_in[at, :], sin_in[at, :])
                qbuf[h, 0, at, :lanes] = nope
                qbuf[h, 1, at, :lanes] = nope
                qbuf[h, 0, at, lanes:] = rot.astype(jnp.bfloat16)
                qbuf[h, 1, at, lanes:] = pltpu.roll(rot, 64, 1).astype(jnp.bfloat16)
            return carry

        lax.fori_loop(0, length // pt, make_queries, 0)

        factor = QK ** (-0.5) * 1.4426950408889634

        def attend(src, first, diagonal):
            knope = [kv[src, s * half : (s + 1) * half, :] for s in range(2)]
            krot = kv[src, 2 * length : bundle, :]
            keys = [jnp.concatenate([knope[s], krot], axis=1) for s in range(2)]
            vals = kv[src, length : 2 * length, :]

            def tile(i, carry):
                at = pl.ds(pl.multiple_of(i * qt, qt), qt)
                outs = []
                for h in range(heads):
                    scores = jnp.concatenate(
                        [split_dot(qbuf[h, s, at, :], keys[s], NT) for s in range(2)], axis=1
                    )
                    scores = scores * factor
                    if diagonal:
                        row = lax.broadcasted_iota(jnp.int32, scores.shape, 0) + i * qt
                        col = lax.broadcasted_iota(jnp.int32, scores.shape, 1)
                        scores = jnp.where(col <= row, scores, -1e30)
                    top = jnp.max(scores, axis=-1, keepdims=True)
                    if not first:
                        old = peak[h, at, :]
                        top = jnp.maximum(old[:, :1], top)
                    weight = jnp.exp2(scores - top)
                    sums = jnp.sum(weight, axis=-1, keepdims=True)
                    part_out = split_dot(weight.astype(jnp.bfloat16), vals, NN)
                    if first:
                        total[h, at, :] = jnp.broadcast_to(sums, (qt, lanes))
                        outs.append((part_out, None))
                    else:
                        fade = jnp.exp2(old[:, :1] - top)
                        total[h, at, :] = total[h, at, :] * fade + sums
                        outs.append((part_out, fade))
                    peak[h, at, :] = jnp.broadcast_to(top, (qt, lanes))
                new, fade = outs[0]
                for h in range(1, heads):
                    new = jnp.where(lane >= h * VH, outs[h][0], new)
                    if not first:
                        fade = jnp.where(lane >= h * VH, outs[h][1], fade)
                acc[at, :] = new if first else acc[at, :] * fade + new
                return carry

            lax.fori_loop(0, length // qt, tile, 0)

        attend(sp, True, True)

        def visit(step, carry):
            src = sp - step

            @pl.when(src >= 0)
            def _():
                remote(
                    kv.at[src], kv.at[src], kv_s.at[src], kv_r.at[src], place.sp_id(src)
                ).wait_recv()
                attend(src, False, False)

            return carry

        lax.fori_loop(1, n_sp, visit, 0)

        for block in range(n_tp):
            at = pl.ds(block * tok, tok)
            bottom = total[0, at, :]
            for h in range(1, heads):
                bottom = jnp.where(lane >= h * VH, total[h, at, :], bottom)
            att[block % 2, (block // 2) * tok : (block // 2 + 1) * tok, :] = (
                acc[at, :] / bottom
            ).astype(jnp.bfloat16)
        att_copies = []
        for step in range(1, n_tp):
            dst = lax.rem(tp + step, n_tp)
            att_copies.append(
                push(
                    att.at[lax.rem(dst, 2)],
                    gath.at[tp],
                    att_s.at[step],
                    att_r.at[step],
                    (sp, dst),
                )
            )
        own = pltpu.make_async_copy(att.at[core], gath.at[tp], local_sem.at[1])
        own.start()

        for copy in meta_copies:
            copy.wait_recv()
        meta = metabuf[...].reshape(part, lanes)
        slot_id = lax.broadcasted_iota(jnp.int32, (part, rows), 1).astype(jnp.float32)
        for e in range(n_sp):
            hit = meta[:, e : e + 1] == slot_id
            mixer[e] = jnp.where(hit, meta[:, 64 + e : 65 + e], 0.0).astype(jnp.bfloat16)
        for copy in res_copies:
            copy.wait_recv()
        local.wait()
        load_w.wait()
        own.wait()
        for copy in att_copies:
            copy.wait_recv()

        square = None
        for t in range(n_tp):
            block = gath[t].astype(jnp.float32)
            square = block * block if square is None else square + block * block
        scale = lax.rsqrt(jnp.sum(square, axis=-1, keepdims=True) / att_width + epsilon)
        for t in range(n_tp):
            normed[:, t * lanes : (t + 1) * lanes] = (
                gath[t].astype(jnp.float32) * scale * outg[t]
            ).astype(jnp.bfloat16)
        ct = 512
        square = None
        for c in range(D // ct):
            cols = slice(c * ct, (c + 1) * ct)
            values = split_dot(normed[...], wbuf[:, cols], NN) + resbuf[:, :, cols].reshape(
                part, ct
            ).astype(jnp.float32)
            mid[:, cols] = values
            more = jnp.sum(values * values, axis=-1, keepdims=True)
            square = more if square is None else square + more
        scale = lax.rsqrt(square / D + epsilon)
        for c in range(D // ct):
            cols = slice(c * ct, (c + 1) * ct)
            ffn[:, cols] = (mid[:, cols] * scale * ffng[0:1, cols]).astype(jnp.bfloat16)
        mid_out[...] = mid[pl.ds(pl.multiple_of(z * tok, tok), tok), :]
        for e in range(n_sp):
            hit = jnp.where(meta[:, e : e + 1] == slot_id, 1.0, 0.0).astype(jnp.bfloat16)
            for c in range(D // ct):
                cols = slice(c * ct, (c + 1) * ct)
                out_rows[e, :, cols] = split_dot(hit, ffn[:, cols], TN).astype(jnp.bfloat16)

        for copy in meta_copies + res_copies + att_copies:
            copy.wait_send()
        for step in range(1, n_sp):
            dst = sp + n_sp - step

            @pl.when(dst < n_sp)
            def _(dst=dst):
                remote(mine, mine, kv_s.at[dst], kv_r.at[sp], place.sp_id(dst)).wait_send()

    dma = pltpu.SemaphoreType.DMA
    bf, f4 = jnp.bfloat16, jnp.float32
    specs = [vmem()] * 9 + [pl.BlockSpec(memory_space=pl.ANY)] + [vmem()] * 6
    return pl.pallas_call(
        kernel,
        out_shape=(
            jax.ShapeDtypeStruct((n_sp, rows, D), bf),
            jax.ShapeDtypeStruct((n_sp, part, rows), bf),
            jax.ShapeDtypeStruct((tok, D), f4),
        ),
        in_specs=specs,
        out_specs=(vmem(),) * 3,
        scratch_shapes=[
            pltpu.VMEM((heads, 2, length, 2 * lanes), bf),
            pltpu.VMEM((n_sp, bundle, lanes), bf),
            pltpu.VMEM((heads, length, lanes), f4),
            pltpu.VMEM((heads, length, lanes), f4),
            pltpu.VMEM((length, lanes), f4),
            pltpu.VMEM((2, part, lanes), bf),
            pltpu.VMEM((n_tp, part, lanes), bf),
            pltpu.VMEM((part, n_tp * lanes), bf),
            pltpu.VMEM(out_weight.shape, bf),
            pltpu.VMEM((n_z, tok, D), bf),
            pltpu.VMEM((n_z, tok, lanes), f4),
            pltpu.VMEM((part, D), f4),
            pltpu.VMEM((part, D), bf),
            dma((1,)),
            dma((2,)),
            dma((n_sp,)),
            dma((n_sp,)),
            dma((n_z,)),
            dma((n_z,)),
            dma((n_z,)),
            dma((n_z,)),
            dma((n_tp,)),
            dma((n_tp,)),
        ],
        compiler_params=pltpu.CompilerParams(
            collective_id=0, has_side_effects=True, vmem_limit_bytes=60 << 20
        ),
        name="front",
    )(
        queries, latent, rot_key, lat_gain, key_up, value_up, q_gain, k_gain, out_gain,
        out_weight, residual, ffn_gain, routes, weights, cosine, sine,
    )


def packed_gain(gain, heads):
    nope = jnp.tile(gain[:NOPE], 2)
    rot = jnp.concatenate([jnp.tile(gain[NOPE:], heads), jnp.zeros((128 - heads * ROPE,))])
    return jnp.concatenate([nope, rot])[None, :]


def shards(
    queries, latent, rot_key, latent_gain, key_up, value_up, query_gain, key_gain, out_gain,
    out_weight, residual, ffn_gain, routes, route_weights, expert_gate, expert_up, expert_down,
):
    length = queries.shape[0]
    heads = key_up.shape[1] // NOPE
    n_sp = lax.axis_size("sp")
    n_tp = lax.axis_size("tp")
    n_z = n_tp // 2
    width = heads * VH
    first = lax.axis_index("sp") * length
    positions = (first + jnp.arange(length, dtype=jnp.int32)).astype(jnp.float32)
    inverse = rope_base ** (-jnp.arange(0, ROPE, 2, dtype=jnp.float32) / ROPE)
    angles = positions[:, None] * jnp.tile(inverse, 128 // (ROPE // 2))[None, :]
    out_gain = out_gain.reshape(n_tp, 1, width)
    if width < 128:
        spare = 128 - width
        key_up = jnp.pad(key_up, ((0, 0), (0, spare)))
        value_up = jnp.pad(value_up, ((0, 0), (0, spare)))
        out_gain = jnp.pad(out_gain, ((0, 0), (0, 0), (0, spare)))
        out_weight = jnp.pad(
            out_weight.reshape(n_tp, width, D), ((0, 0), (0, spare), (0, 0))
        ).reshape(n_tp * 128, D)
    outbound, mixer, middle = front(
        queries, latent, rot_key, latent_gain[None, :], key_up, value_up,
        packed_gain(query_gain, heads), packed_gain(key_gain, heads), out_gain, out_weight,
        residual, ffn_gain[None, :], routes, route_weights, jnp.cos(angles), jnp.sin(angles),
        n_sp, n_z, n_tp * width,
    )
    rows = outbound.shape[1]
    arrived = send_rows(outbound, n_sp, n_z)
    row_block = arrived.reshape(2 * n_sp * rows, D)
    gate_pre = jnp.dot(row_block, expert_gate[0], preferred_element_type=jnp.float32)
    up_pre = jnp.dot(row_block, expert_up[0], preferred_element_type=jnp.float32)
    hidden = (jax.nn.silu(gate_pre) * up_pre).astype(jnp.bfloat16)
    return return_rows(
        hidden.reshape(2, n_sp, rows, -1), expert_down[0], mixer, middle, n_sp, n_z
    )


def solution(mesh):
    return jax.shard_map(
        shards,
        mesh=mesh,
        in_specs=(
            P("sp", "tp"),
            P("sp", None),
            P("sp", None),
            P(),
            P(None, "tp"),
            P(None, "tp"),
            P(),
            P(),
            P(),
            P(),
            P(("sp", "tp"), None),
            P(),
            P(("sp", "tp"), None),
            P(("sp", "tp"), None),
            P("sp", None, "tp"),
            P("sp", None, "tp"),
            P("sp", "tp", None),
        ),
        out_specs=P(("sp", "tp"), None),
        check_vma=False,
    )
```

time: 167 us -> 143 us (0.86)
  matrix products: 15.5 us -> 6.25 us
  Pallas kernels: 131 us -> 123 us
  other arithmetic: 9.79 us -> 2.46 us
  local copies, waits for them, and re-layouts: 9.3 us -> 11.1 us
    dot_general x6 -> x0, matrix products: 9.29 us -> none  [the longest x1 3.58 us: shards(): mixed = jnp.dot(normed_rows, out_weight, preferred_element_type=jnp.float32)]
    pallas_call x1, Pallas kernels: 41.3 us -> 33.5 us  [send_rows(): pl.pallas_call(kernel, out_shape=jax.ShapeDtypeStruct((2, n_sp, rows, D),...]
    reduce_sum x8 -> x0, other arithmetic: 4.8 us -> none  [the longest x4 3.54 us: rms_scale(): jnp.mean(values * values, axis=-1, keepdims=True) + epsilon]
    unnamed x28 -> x11, local copies, waits for them, and re-layouts: 3.64 us -> 7.83 us
    convert_element_type x6 -> x1, other arithmetic: 2.3 us -> 0.01 us  [shards(): (first + jnp.arange(length, dtype=jnp.int32)).astype(jnp.float32)]
    convert_element_type x4 -> x0, local copies, waits for them, and re-layouts: 1.94 us -> none  [the longest x1 1 us: shards(): jnp.sum(jnp.where(hits, part_weights[:, :, None], 0.0), axis=1)]
    sin x0 -> x1, other arithmetic: none -> 1.79 us  [shards(): jnp.sin(angles)]
    pallas_call x2 -> x1, Pallas kernels: 47.1 us -> 46.3 us  [front(): pl.pallas_call(kernel, out_shape=(jax.ShapeDtypeStruct((n_sp, rows, D), b...]
where the time goes in v1:
time: 143 us; the launch traced here: 142 us
  Pallas kernels  123 us (86%)
  local copies, waits for them, and re-layouts  11.1 us (8%)
  matrix products  6.25 us (4%)
  other arithmetic  2.46 us (2%)
    pallas_call x1, Pallas kernels, front(): pl.pallas_call(kernel, out_shape=(jax.ShapeDtypeStruct((n_sp, rows, D), b...  46.3 us
    pallas_call x1, Pallas kernels, return_rows(): pl.pallas_call(kernel, out_shape=jax.ShapeDtypeStruct((tok, D), jnp.bfloa...  42.7 us
    pallas_call x1, Pallas kernels, send_rows(): pl.pallas_call(kernel, out_shape=jax.ShapeDtypeStruct((2, n_sp, rows, D),...  33.5 us
    unnamed x11, local copies, waits for them, and re-layouts  7.83 us
    dot_general x1, matrix products, shards(): jnp.dot(row_block, expert_gate[0], preferred_element_type=jnp.float32)  3.89 us

profile of v1, /device:TPU:0, one launch (start us, length us, event | category | flops | bytes accessed | tf_op | source)
XLA Modules:
  0.0 142.4 jit_solution(17251417831965445486)
XLA Ops:
  0.0 0.0 copy-start
  0.0 0.8 slice.13
  0.8 0.1 tile.21
  0.9 0.7 slice.15
  1.6 0.1 tile.49
  1.7 0.7 tile.22
  2.4 0.1 tile.23
  2.5 0.7 tile.18
  3.1 0.1 tile.19
  3.2 0.7 pad_maximum_fusion
  3.9 0.1 mul.35
  4.0 1.4 copy.20.routes_in
  5.3 1.4 copy.21.weights_in
  6.7 1.5 %copy.19.rot_in = bf16[512,32]{1,0:T(8,128)(2,1)} copy(bf16[512,32]{0,1:T(8,128)(2,1)} %param.19) | data formatting | bytes 65536 | tf_op args[2]
  8.2 1.8 %copy.18.q_in = bf16[512,192]{1,0:T(8,128)(2,1)} copy(bf16[512,192]{0,1:T(8,128)(2,1)} %param.17) | data formatting | bytes 393216 | tf_op args[0]
  10.0 1.8 %multiply_sine_fusion = (f32[512,128]{1,0:T(8,128)}, f32[512,128]{1,0:T(8,128)}) fusion(f32[128]{0:T(128)S(1)} %mul.35, f32[512]{0:T(512)S(1)} %add_convert_fusion), kind=kLoop, calls=%fused_computation.5 | loop fusion | flops 65536 | bytes 526848 | tf_op jit(solution)/shard_map/sin | solution.py:649
  11.8 46.3 %front.1 = (bf16[4,144,2048]{2,1,0:T(8,128)(2,1)}, bf16[4,256,144]{2,1,0:T(8,128)(2,1)}, f32[64,2048]{1,0:T(8,128)}) custom-call(bf16[512,192]{1,0:T(8,128)(2,1)} %copy.18.q_in, bf16[512,512]{1,0:T(8,128)(2,1)} %lat_in.1, bf16[512,32]{1,0:T(8,128)(2,1)} %copy.19.rot_in, f32[1,512]{1,0:T(1,128)} %bitcast.26, bf16[512,128]{1,0:T(8,128)(2,1)} %kup.1, ...), custom_call_target="tpu_custom_call" | custom-call | tf_op jit(solution)/shard_map/front/pallas_call | solution.py:573
  58.1 33.5 %send_rows.1 = bf16[2,4,144,2048]{3,2,1,0:T(8,128)(2,1)} custom-call(bf16[4,144,2048]{2,1,0:T(8,128)(2,1)} %get-tuple-element.8.x_ref), custom_call_target="tpu_custom_call" | custom-call | tf_op jit(solution)/shard_map/send_rows/pallas_call | solution.py:134
  91.6 0.0 copy-done
  91.6 0.0 copy-start.1
  91.6 0.0 copy-start.2
  91.7 3.9 %fusion.2 = f32[1152,256]{1,0:T(8,128)S(1)} fusion(bf16[1152,2048]{1,0:T(8,128)(2,1)} %bitcast.18, bf16[1,2048,256]{2,1,0:T(8,128)(2,1)S(1)} %copy-done), kind=kOutput, calls=%fused_computation.3 | convolution fusion | flops 1207959552 | bytes 6946816 | tf_op jit(solution)/shard_map/dot_general | solution.py:655
  95.6 0.0 copy-done.1
  95.6 0.1 copy-done.2
  95.7 2.4 %fusion = bf16[1152,256]{1,0:T(8,128)(2,1)} fusion(bf16[1152,2048]{1,0:T(8,128)(2,1)S(1)} %bitcast.19, f32[1152,256]{1,0:T(8,128)S(1)} %fusion.2, bf16[1,2048,256]{2,1,0:T(8,128)(2,1)S(1)} %copy-done.2), kind=kOutput, calls=%fused_computation.1 | convolution fusion | flops 1209729024 | bytes 7536640 | tf_op jit(solution)/shard_map/dot_general | solution.py:656
  98.1 42.7 %return_rows.1 = bf16[64,2048]{1,0:T(8,128)(2,1)} custom-call(bf16[2,4,144,256]{3,2,1,0:T(8,128)(2,1)} %bitcast.21, bf16[256,2048]{1,0:T(8,128)(2,1)} %bitcast.20, bf16[4,256,144]{2,1,0:T(8,128)(2,1)} %get-tuple-element.9.mix_ref, f32[64,2048]{1,0:T(8,128)} %get-tuple-element.10.mid_ref), custom_call_target="tpu_custom_call" | custom-call | tf_op jit(solution)/shard_map/return_rows/pallas_call | solution.py:236
  140.8 1.7 %copy.23 = bf16[64,2048]{1,0:T(8,128)(2,1)} copy(bf16[64,2048]{1,0:T(8,128)(2,1)} %return_rows.1) | data formatting | bytes 524288
  (6 shorter events, 0.0 us)
Async XLA Ops:
  0.0 91.6 %copy-start = (bf16[1,2048,256]{2,1,0:T(8,128)(2,1)S(1)}, bf16[1,2048,256]{2,1,0:T(8,128)(2,1)}, u32[]{:S(2)}) copy-start(bf16[1,2048,256]{2,1,0:T(8,128)(2,1)} %param.31) | copy-start | bytes 3145732
  91.6 3.9 %copy-start.1 = (bf16[2,4,144,2048]{3,2,1,0:T(8,128)(2,1)S(1)}, bf16[2,4,144,2048]{3,2,1,0:T(8,128)(2,1)}, u32[]{:S(2)}) copy-start(bf16[2,4,144,2048]{3,2,1,0:T(8,128)(2,1)} %send_rows.1) | copy-start | bytes 14155780
  91.6 4.1 %copy-start.2 = (bf16[1,2048,256]{2,1,0:T(8,128)(2,1)S(1)}, bf16[1,2048,256]{2,1,0:T(8,128)(2,1)}, u32[]{:S(2)}) copy-start(bf16[1,2048,256]{2,1,0:T(8,128)(2,1)} %param.32) | copy-start | bytes 3145732

commit v2 on v1

--- a/solution.py
+++ b/solution.py
@@ -1,5 +1,6 @@
 import jax
 import jax.numpy as jnp
+import numpy as np
 from jax import lax
 from jax.experimental import pallas as pl
 from jax.experimental.pallas import tpu as pltpu
@@ -74,178 +75,267 @@
     return pl.BlockSpec(memory_space=pltpu.VMEM)
 
 
-def send_rows(x, n_sp, n_z):
-    rows, shared = x.shape[1], D // 4
+def flip(value, bits):
+    shift = 1
+    while shift <= bits:
+        if bits & shift:
+            value = value + shift * (1 - 2 * lax.rem(lax.div(value, shift), 2))
+        shift *= 2
+    return value
+
+
+CHUNKS = 8
+PIECES = 3
+
+
+def experts(outbound, mixer, middle, gate, up, down, n_sp, n_z):
+    rows = outbound.shape[1]
+    tok = middle.shape[0]
+    width = D // CHUNKS
+    hidden = gate.shape[1]
+    shared = D // 4
     half = (D - shared) // 2
-
-    def kernel(x_ref, o_ref, local_sem, *sems):
+    piece = half // PIECES
+    phases = [[1, 2]] + [[k] for k in range(3, n_sp)] if n_sp > 2 else [[1]]
+
+    def kernel(
+        x_in, mix_in, mid_in, gate_hbm, up_hbm, down_hbm, o_ref,
+        gbuf, ubuf, dbuf, xbuf, hid, ybuf, pbuf, sbuf, rbuf, cbuf, fbuf,
+        w_sem, a_s, a_r, b_s, b_r, t_s, t_r, pa_s, pa_r, pb_s, pb_r, pt_s, pt_r, po_s, po_r,
+        y_s, y_r, sp_s, sp_r, z_s, z_r,
+    ):
         place = Place(n_sp, n_z)
-        core, me = place.core, place.sp
+        core, z, me = place.core, place.z, place.sp
+        loads = []
+        for i, (src, dst) in enumerate(((gate_hbm, gbuf), (up_hbm, ubuf), (down_hbm, dbuf))):
+            load = pltpu.make_async_copy(src, dst, w_sem.at[i])
+            load.start()
+            loads.append(load)
         place.barrier(True, True)
-        side = lax.rem(place.z, 2)
-        twin = place.z_id(place.z + 1 - 2 * side)
-        mine = pl.ds(pl.multiple_of(shared + side * half, 128), half)
-        other = pl.ds(pl.multiple_of(shared + (1 - side) * half, 128), half)
+        side = lax.rem(z, 2)
+        twin = place.z_id(z + 1 - 2 * side)
+        partner = place.partner()
         both = pl.ds(0, shared)
+
+        def strip(which, p):
+            return pl.ds(pl.multiple_of(shared + which * half + p * piece, 128), piece)
+
         copies = []
 
-        def push(kind, step, src, dst, device):
-            copy = remote(src, dst, sems[2 * kind].at[step], sems[2 * kind + 1].at[step], device)
+        def push(src, dst, send, recv, device):
+            copy = remote(src, dst, send, recv, device)
             copy.start()
             copies.append(copy)
             return copy
 
-        split, direct, swapped = {}, {}, {}
-        for step in range(1, n_sp):
-            dst = place.sp_peer(step)
-            split[step] = push(
-                0, step, x_ref.at[dst, :, mine], o_ref.at[core, me, :, mine], place.sp_id(dst)
-            )
-        for step in range(1, n_sp):
-            dst = place.sp_peer(step)
-            direct[step] = push(
-                1, step, x_ref.at[dst, :, both], o_ref.at[core, me, :, both], place.sp_id(dst)
-            )
-        local = pltpu.make_async_copy(x_ref.at[me], o_ref.at[core, me], local_sem.at[0])
-        local.start()
-        last = [push(3, 0, x_ref.at[me], o_ref.at[core, me], place.partner())]
-        for step in range(1, n_sp):
-            src = lax.rem(me - step + n_sp, n_sp)
-            piece = o_ref.at[core, src, :, mine]
-            split[step].wait_recv()
-            swapped[step] = push(2, step, piece, piece, twin)
-            last.append(push(3, step, piece, piece, place.partner()))
-        for step in range(1, n_sp):
-            src = lax.rem(me - step + n_sp, n_sp)
-            piece = o_ref.at[core, src, :, both]
-            direct[step].wait_recv()
-            last.append(push(4, step, piece, piece, place.partner()))
-        for step in range(1, n_sp):
-            src = lax.rem(me - step + n_sp, n_sp)
-            piece = o_ref.at[core, src, :, other]
-            swapped[step].wait_recv()
-            last.append(push(5, step, piece, piece, place.partner()))
-        for copy in last:
-            copy.wait_recv()
+        own_in = push(
+            x_in.at[me], xbuf.at[core, me], po_s.at[0], po_r.at[0], partner
+        )
+        strips, shares, swaps, to_pair = {}, {}, {}, {k: [] for k in range(n_sp)}
+        for ks in phases:
+            for p in range(PIECES):
+                for k in ks:
+                    dst = flip(me, k)
+                    cols = strip(side, p)
+                    strips[k, p] = push(
+                        x_in.at[dst, :, cols], xbuf.at[core, me, :, cols],
+                        a_s.at[k, p], a_r.at[k, p], place.sp_id(dst),
+                    )
+            for k in ks:
+                dst = flip(me, k)
+                shares[k] = push(
+                    x_in.at[dst, :, both], xbuf.at[core, me, :, both],
+                    b_s.at[k], b_r.at[k], place.sp_id(dst),
+                )
+
+        def forward_strip(k, p):
+            block = xbuf.at[core, flip(me, k), :, strip(side, p)]
+            strips[k, p].wait_recv()
+            swaps[k, p] = push(block, block, t_s.at[k, p], t_r.at[k, p], twin)
+            to_pair[k].append(push(block, block, pa_s.at[k, p], pa_r.at[k, p], partner))
+
+        def forward_share(k):
+            block = xbuf.at[core, flip(me, k), :, both]
+            shares[k].wait_recv()
+            to_pair[k].append(push(block, block, pb_s.at[k], pb_r.at[k], partner))
+
+        def forward_swap(k, p):
+            block = xbuf.at[core, flip(me, k), :, strip(1 - side, p)]
+            swaps[k, p].wait_recv()
+            to_pair[k].append(push(block, block, pt_s.at[k, p], pt_r.at[k, p], partner))
+
+        def expert(x_ref, h_ref):
+            g = jnp.dot(x_ref[...], gbuf[...], preferred_element_type=jnp.float32)
+            u = jnp.dot(x_ref[...], ubuf[...], preferred_element_type=jnp.float32)
+            h_ref[...] = (g / (1.0 + jnp.exp(-g)) * u).astype(jnp.bfloat16)
+
+        def column(q):
+            return pl.ds(pl.multiple_of(q * width, width), width)
+
+        def pair_copy(k, q):
+            src = flip(me, k)
+            return remote(
+                ybuf.at[src, :, column(q)], pbuf.at[src, :, column(q)],
+                y_s.at[k, q], y_r.at[k, q], partner,
+            )
+
+        def back_copy(k, q):
+            src = flip(me, k)
+            return remote(
+                sbuf.at[src, :, column(q)], rbuf.at[me, :, column(q)],
+                sp_s.at[k, q], sp_r.at[k, q], place.sp_id(src),
+            )
+
+        def expert_own(k):
+            src = flip(me, k)
+            expert(x_in.at[me] if k == 0 else xbuf.at[core, src], hid.at[core, src])
+
+        def expert_pair(k):
+            src = flip(me, k)
+            if k == 0:
+                own_in.wait_recv()
+            for copy in to_pair[k]:
+                copy.wait_recv()
+            expert(xbuf.at[1 - core, src], hid.at[1 - core, src])
+
+            def body(q, carry):
+                ybuf[src, :, column(q)] = jnp.dot(
+                    hid[1 - core, src], dbuf[:, column(q)], preferred_element_type=jnp.float32
+                ).astype(jnp.bfloat16)
+                pair_copy(k, q).start()
+                return carry
+
+            lax.fori_loop(0, CHUNKS, body, 0)
+
+        def finish(ks):
+            def body(q, carry):
+                for k in ks:
+                    src = flip(me, k)
+                    own = jnp.dot(
+                        hid[core, src], dbuf[:, column(q)], preferred_element_type=jnp.float32
+                    )
+                    pair_copy(k, q).wait_recv()
+                    total = (own + pbuf[src, :, column(q)].astype(jnp.float32)).astype(
+                        jnp.bfloat16
+                    )
+                    if k == 0:
+                        rbuf[src, :, column(q)] = total
+                    else:
+                        sbuf[src, :, column(q)] = total
+                        back_copy(k, q).start()
+                return carry
+
+            lax.fori_loop(0, CHUNKS, body, 0)
+
+        def arrivals(ks):
+            steps = []
+            for p in range(PIECES):
+                steps.append(lambda p=p: [forward_strip(k, p) for k in ks])
+            steps.append(lambda: [forward_share(k) for k in ks])
+            return steps
+
+        for load in loads[:2]:
+            load.wait()
+        waiting = arrivals(phases[0])
+        expert_own(0)
+        waiting.pop(0)()
+        loads[2].wait()
+        expert_pair(0)
+        waiting.pop(0)()
+        finish([0])
+        for index, ks in enumerate(phases):
+            while waiting:
+                waiting.pop(0)()
+            for p in range(PIECES):
+                for k in ks:
+                    forward_swap(k, p)
+            waiting = arrivals(phases[index + 1]) if index + 1 < len(phases) else []
+            for k in ks:
+                expert_own(k)
+            if waiting:
+                waiting.pop(0)()
+            for k in ks:
+                expert_pair(k)
+                if waiting:
+                    waiting.pop(0)()
+            finish(ks)
+
+        def z_copy(q, step):
+            dst = place.z_peer(step)
+            return remote(
+                cbuf.at[dst, :, column(q)], fbuf.at[z, :, column(q)],
+                z_s.at[q, step], z_r.at[q, step], place.z_id(dst),
+            )
+
+        def combine(q, carry):
+            for k in range(1, n_sp):
+                back_copy(k, q).wait_recv()
+            total = None
+            for src in range(n_sp):
+                more = split_dot(mix_in[src], rbuf[src, :, column(q)], TN)
+                total = more if total is None else total + more
+            cbuf[:, :, column(q)] = total.astype(jnp.bfloat16).reshape(n_z, tok, width)
+            for step in range(1, n_z):
+                z_copy(q, step).start()
+            return carry
+
+        lax.fori_loop(0, CHUNKS, combine, 0)
+
+        def close(q, carry):
+            total = mid_in[:, column(q)] + cbuf[z, :, column(q)].astype(jnp.float32)
+            for step in range(1, n_z):
+                z_copy(q, step).wait_recv()
+                total += fbuf[lax.rem(z - step + n_z, n_z), :, column(q)].astype(jnp.float32)
+            o_ref[:, column(q)] = total.astype(jnp.bfloat16)
+            return carry
+
+        lax.fori_loop(0, CHUNKS, close, 0)
+
+        def drain(q, carry):
+            for k in range(n_sp):
+                pair_copy(k, q).wait_send()
+            for k in range(1, n_sp):
+                back_copy(k, q).wait_send()
+            for step in range(1, n_z):
+                z_copy(q, step).wait_send()
+            return carry
+
         for copy in copies:
             copy.wait_send()
-        local.wait()
-
+        lax.fori_loop(0, CHUNKS, drain, 0)
+
+    dma = pltpu.SemaphoreType.DMA
+    bf = jnp.bfloat16
+    block = pltpu.VMEM((n_sp, rows, D), bf)
+    zblock = pltpu.VMEM((n_z, tok, D), bf)
+    any_spec = pl.BlockSpec(memory_space=pl.ANY)
     return pl.pallas_call(
         kernel,
-        out_shape=jax.ShapeDtypeStruct((2, n_sp, rows, D), x.dtype),
-        in_specs=[vmem()],
+        out_shape=jax.ShapeDtypeStruct((tok, D), bf),
+        in_specs=[vmem()] * 3 + [any_spec] * 3,
         out_specs=vmem(),
-        scratch_shapes=[pltpu.SemaphoreType.DMA((1,))] + [pltpu.SemaphoreType.DMA((n_sp,))] * 12,
-        compiler_params=pltpu.CompilerParams(
-            collective_id=2, has_side_effects=True, vmem_limit_bytes=60 << 20
-        ),
-        name="send_rows",
-    )(x)
-
-
-CHUNKS = 4
-
-
-def return_rows(hidden, down, mixer, middle, n_sp, n_z):
-    rows = hidden.shape[2]
-    tok = middle.shape[0]
-    width = D // CHUNKS
-
-    def kernel(h_ref, w_ref, mix_ref, mid_ref, o_ref, ybuf, pbuf, sbuf, rbuf, cbuf, fbuf, *sems):
-        pair_s, pair_r, sp_s, sp_r, z_s, z_r = sems
-        place = Place(n_sp, n_z)
-        core = place.core
-        place.barrier(True, True)
-        pairs, sends, zsends = {}, {}, {}
-        order = list(range(1, n_sp)) + [0]
-        for q in range(CHUNKS):
-            cols = pl.ds(q * width, width)
-            for step in order:
-                dst = place.sp_peer(step)
-                ybuf[dst, :, cols] = jnp.dot(
-                    h_ref[1 - core, dst], w_ref[:, cols], preferred_element_type=jnp.float32
-                ).astype(jnp.bfloat16)
-                copy = remote(
-                    ybuf.at[dst, :, cols],
-                    pbuf.at[dst, :, cols],
-                    pair_s.at[q, step],
-                    pair_r.at[q, step],
-                    place.partner(),
-                )
-                copy.start()
-                pairs[q, step] = copy
-        for q in range(CHUNKS):
-            cols = pl.ds(q * width, width)
-            for step in order:
-                dst = place.sp_peer(step)
-                own = jnp.dot(
-                    h_ref[core, dst], w_ref[:, cols], preferred_element_type=jnp.float32
-                )
-                pairs[q, step].wait_recv()
-                total = (own + pbuf[dst, :, cols].astype(jnp.float32)).astype(jnp.bfloat16)
-                if step == 0:
-                    rbuf[dst, :, cols] = total
-                else:
-                    sbuf[dst, :, cols] = total
-                    copy = remote(
-                        sbuf.at[dst, :, cols],
-                        rbuf.at[place.sp, :, cols],
-                        sp_s.at[q, step],
-                        sp_r.at[q, step],
-                        place.sp_id(dst),
-                    )
-                    copy.start()
-                    sends[q, step] = copy
-        for q in range(CHUNKS):
-            cols = pl.ds(q * width, width)
-            for step in range(1, n_sp):
-                sends[q, step].wait_recv()
-            combined = jnp.zeros((n_z * tok, width), jnp.float32)
-            for src in range(n_sp):
-                combined += jnp.dot(
-                    mix_ref[src], rbuf[src, :, cols], preferred_element_type=jnp.float32
-                )
-            cbuf[:, :, cols] = combined.astype(jnp.bfloat16).reshape(n_z, tok, width)
-            for step in range(1, n_z):
-                dst = place.z_peer(step)
-                copy = remote(
-                    cbuf.at[dst, :, cols],
-                    fbuf.at[place.z, :, cols],
-                    z_s.at[q, step],
-                    z_r.at[q, step],
-                    place.z_id(dst),
-                )
-                copy.start()
-                zsends[q, step] = copy
-        for q in range(CHUNKS):
-            cols = pl.ds(q * width, width)
-            total = mid_ref[:, cols] + cbuf[place.z, :, cols].astype(jnp.float32)
-            for step in range(1, n_z):
-                src = lax.rem(place.z - step + n_z, n_z)
-                zsends[q, step].wait_recv()
-                total += fbuf[src, :, cols].astype(jnp.float32)
-            o_ref[:, cols] = total.astype(jnp.bfloat16)
-        for group in (pairs, sends, zsends):
-            for copy in group.values():
-                copy.wait_send()
-
-    dma = pltpu.SemaphoreType.DMA
-    block = pltpu.VMEM((n_sp, rows, D), jnp.bfloat16)
-    zblock = pltpu.VMEM((n_z, tok, D), jnp.bfloat16)
-    return pl.pallas_call(
-        kernel,
-        out_shape=jax.ShapeDtypeStruct((tok, D), jnp.bfloat16),
-        in_specs=[vmem()] * 4,
-        out_specs=vmem(),
-        scratch_shapes=[block, block, block, block, zblock, zblock]
-        + [dma((CHUNKS, n_sp))] * 4
+        scratch_shapes=[
+            pltpu.VMEM(gate.shape, bf),
+            pltpu.VMEM(up.shape, bf),
+            pltpu.VMEM(down.shape, bf),
+            pltpu.VMEM((2, n_sp, rows, D), bf),
+            pltpu.VMEM((2, n_sp, rows, hidden), bf),
+            block, block, block, block, zblock, zblock,
+            dma((3,)),
+        ]
+        + [dma((n_sp, PIECES))] * 2
+        + [dma((n_sp,))] * 2
+        + [dma((n_sp, PIECES))] * 4
+        + [dma((n_sp,))] * 2
+        + [dma((n_sp, PIECES))] * 2
+        + [dma((1,))] * 2
+        + [dma((n_sp, CHUNKS))] * 4
         + [dma((CHUNKS, n_z))] * 2,
         compiler_params=pltpu.CompilerParams(
-            collective_id=3, has_side_effects=True, vmem_limit_bytes=60 << 20
+            collective_id=1, has_side_effects=True, vmem_limit_bytes=62 << 20
         ),
-        name="return_rows",
-    )(hidden, down, mixer, middle)
+        name="experts",
+    )(outbound, mixer, middle, gate, up, down)
 
 
 def split_dot(a, b, dims):
@@ -259,10 +349,9 @@
 
 def front(
     queries, latent, rot_key, lat_gain, key_up, value_up, q_gain, k_gain, out_gain,
-    out_weight, residual, ffn_gain, routes, weights, cosine, sine, n_sp, n_z, width,
+    out_weight, residual, ffn_gain, routes, weights, n_sp, n_z, width,
 ):
-    length = queries.shape[0]
-    heads = queries.shape[1] // QK
+    heads, length = queries.shape[0] // QK, queries.shape[1]
     n_tp = 2 * n_z
     tok = residual.shape[0]
     part = n_z * tok
@@ -274,11 +363,15 @@
     att_width = width
     qt = 256
     pt = 128
+    per = lanes // tok
+    named_rows = -(-n_sp // 8) * 8
+    freqs = ROPE // 2
+    inverse = np.float32(rope_base) ** (-np.arange(0, ROPE, 2, dtype=np.float32) / np.float32(ROPE))
 
     def kernel(
         q_in, lat_in, rot_in, latg, kup, vup, qg, kg, outg, w_hbm, res_in, ffng, routes_in,
-        weights_in, cos_in, sin_in, out_rows, mixer, mid_out,
-        qbuf, kv, peak, total, acc, att, gath, normed, wbuf, resbuf, metabuf, mid, ffn,
+        weights_in, out_rows, mixer, mid_out,
+        table, gains, tokens, qbuf, kv, peak, total, acc, att, gath, normed, wbuf, resbuf, metabuf, mid, ffn,
         w_sem, local_sem, kv_s, kv_r, res_s, res_r, meta_s, meta_r, att_s, att_r,
     ):
         place = Place(n_sp, n_z)
@@ -295,22 +388,68 @@
                 sem, inc=1, device_id=place.sp_id(place.sp_peer(step)), device_id_type=MESH_ID
             )
 
-        lane_id = lax.broadcasted_iota(jnp.int32, (tok, lanes), 1)
-        r0, r1 = routes_in[:, 0:1], routes_in[:, 1:2]
-        named0, named1 = lane_id == r0, lane_id == r1
+        tokens[0:1, :] = jnp.full((1, lanes), -1.0, jnp.float32)
+        tokens[1:2, :] = jnp.full((1, lanes), -1.0, jnp.float32)
+        tokens[0:TOPK, :tok] = routes_in[...].astype(jnp.float32)
+        tokens[2:4, :tok] = weights_in[...]
+        expert_id = lax.broadcasted_iota(jnp.int32, (named_rows, lanes), 0).astype(jnp.float32)
+        named0 = expert_id == tokens[0:1, :]
+        named1 = expert_id == tokens[1:2, :]
         named = jnp.where(named0 | named1, 1.0, 0.0)
         earlier = jnp.where(
-            lax.broadcasted_iota(jnp.int32, (tok, tok), 1)
-            < lax.broadcasted_iota(jnp.int32, (tok, tok), 0),
+            lax.broadcasted_iota(jnp.int32, (lanes, lanes), 0)
+            < lax.broadcasted_iota(jnp.int32, (lanes, lanes), 1),
             1.0,
             0.0,
         ).astype(jnp.bfloat16)
-        rank = split_dot(earlier, named.astype(jnp.bfloat16), NN)
+        rank = split_dot(named.astype(jnp.bfloat16), earlier, NN)
         slot = jnp.where(named0 | named1, rank + (z * cap).astype(jnp.float32), -1.0)
-        share = jnp.where(named0, weights_in[:, 0:1], 0.0) + jnp.where(
-            named1, weights_in[:, 1:2], 0.0
+        share = jnp.where(named0, tokens[2:3, :], 0.0) + jnp.where(named1, tokens[3:4, :], 0.0)
+        place_by = lax.rem(z, per)
+        for turn_by in range(per):
+
+            @pl.when(place_by == turn_by)
+            def _(turn_by=turn_by):
+                metabuf[z, :named_rows] = pltpu.roll(slot, turn_by * tok, 1) if turn_by else slot
+                metabuf[z, named_rows:] = pltpu.roll(share, turn_by * tok, 1) if turn_by else share
+
+        freq_id = lax.broadcasted_iota(jnp.int32, (freqs, pt), 0)
+        freq = jnp.zeros((freqs, pt), jnp.float32)
+        for i in range(freqs):
+            freq = jnp.where(freq_id == i, float(inverse[i]), freq)
+        spread_by = jnp.where(
+            lax.broadcasted_iota(jnp.int32, (freqs, lanes), 1) % freqs
+            == lax.broadcasted_iota(jnp.int32, (freqs, lanes), 0),
+            1.0,
+            0.0,
         )
-        metabuf[z] = jnp.where(lane_id < 64, slot, pltpu.roll(share, 64, 1))
+
+        def make_table(i, carry):
+            where = lax.broadcasted_iota(jnp.int32, (freqs, pt), 1) + (sp * length + i * pt)
+            angle = where.astype(jnp.float32) * freq
+            at = pl.ds(pl.multiple_of(i * pt, pt), pt)
+            for which, values in enumerate((jnp.cos(angle), jnp.sin(angle))):
+                table[which, at, :] = lax.dot_general(
+                    values, spread_by, (TN, ((), ())), precision=lax.Precision.HIGHEST,
+                    preferred_element_type=jnp.float32,
+                )
+            return carry
+
+        lax.fori_loop(0, length // pt, make_table, 0)
+        for i, gain in enumerate((qg, kg)):
+            gains[4 + i : 5 + i, :] = jnp.zeros((1, lanes), jnp.float32)
+            gains[4 + i : 5 + i, :QK] = gain[...]
+        gain_lane = lax.broadcasted_iota(jnp.int32, (1, lanes), 1)
+        packed = []
+        for i in range(2):
+            raw_gain = gains[4 + i : 5 + i, :]
+            nope_gain = jnp.where(gain_lane < NOPE, raw_gain, pltpu.roll(raw_gain, NOPE, 1))
+            once = jnp.where(gain_lane < ROPE, pltpu.roll(raw_gain, lanes - NOPE, 1), 0.0)
+            rot_gain = once
+            for h in range(1, heads):
+                rot_gain = rot_gain + pltpu.roll(once, h * ROPE, 1)
+            packed.append((nope_gain, rot_gain))
+        (q_nope_gain, q_rot_gain), (k_nope_gain, k_rot_gain) = packed
 
         pl.semaphore_wait(sem, n_tp - 1 + n_sp - 1)
         sends = []
@@ -360,7 +499,7 @@
             nope = split_dot(normed_lat, kup[...], NN).astype(jnp.bfloat16).astype(jnp.float32)
             vals = split_dot(normed_lat, vup[...], NN).astype(jnp.bfloat16)
             kv[sp, pl.ds(pl.multiple_of(length + i * pt, pt), pt), :] = vals
-            rot = split_dot(rot_in[at, :], rot_sel, NN)
+            rot = split_dot(rot_in[:, at], rot_sel, TN)
             square, rot_square = nope * nope, rot * rot
             nope_scale, rot_scale = None, None
             for h in range(heads):
@@ -377,8 +516,8 @@
                 )
                 nope_scale = one if h == 0 else jnp.where(in_nope, one, nope_scale)
                 rot_scale = one if h == 0 else jnp.where(in_rot, one, rot_scale)
-            kv[sp, at, :] = (nope * nope_scale * kg[0:1, :lanes]).astype(jnp.bfloat16)
-            turned = turn(rot * rot_scale * kg[0:1, lanes:], cos_in[at, :], sin_in[at, :])
+            kv[sp, at, :] = (nope * nope_scale * k_nope_gain).astype(jnp.bfloat16)
+            turned = turn(rot * rot_scale * k_rot_gain, table[0, at, :], table[1, at, :])
             return turned
 
         def make_pair(i, carry):
@@ -412,15 +551,14 @@
 
         def make_queries(i, carry):
             at = pl.ds(pl.multiple_of(i * pt, pt), pt)
-            raw = q_in[at, :]
+            raw = q_in[:, at]
             for h in range(heads):
-                spread = split_dot(raw, pickers[h], NN)
+                spread = split_dot(raw, pickers[h], TN)
                 scale = lax.rsqrt(
                     jnp.sum(spread * spread, axis=-1, keepdims=True) / QK + epsilon
                 )
-                spread = spread * scale * qg[0:1, :]
-                nope = spread[:, :lanes].astype(jnp.bfloat16)
-                rot = turn(spread[:, lanes:], cos_in[at, :], sin_in[at, :])
+                nope = (spread[:, :lanes] * scale * q_nope_gain).astype(jnp.bfloat16)
+                rot = turn(spread[:, lanes:] * scale * q_rot_gain, table[0, at, :], table[1, at, :])
                 qbuf[h, 0, at, :lanes] = nope
                 qbuf[h, 1, at, :lanes] = nope
                 qbuf[h, 0, at, lanes:] = rot.astype(jnp.bfloat16)
@@ -515,11 +653,19 @@
 
         for copy in meta_copies:
             copy.wait_recv()
-        meta = metabuf[...].reshape(part, lanes)
-        slot_id = lax.broadcasted_iota(jnp.int32, (part, rows), 1).astype(jnp.float32)
+        pieces = []
+        for first in range(0, n_z, per):
+            piece = metabuf[first]
+            for i in range(1, per):
+                piece = jnp.where(lane >= i * tok, metabuf[first + i], piece)
+            pieces.append(piece)
+        meta = jnp.concatenate(pieces, axis=1)
+        slot_id = lax.broadcasted_iota(jnp.int32, (rows, part), 0).astype(jnp.float32)
         for e in range(n_sp):
-            hit = meta[:, e : e + 1] == slot_id
-            mixer[e] = jnp.where(hit, meta[:, 64 + e : 65 + e], 0.0).astype(jnp.bfloat16)
+            hit = meta[e : e + 1, :] == slot_id
+            mixer[e] = jnp.where(
+                hit, meta[named_rows + e : named_rows + e + 1, :], 0.0
+            ).astype(jnp.bfloat16)
         for copy in res_copies:
             copy.wait_recv()
         local.wait()
@@ -553,10 +699,10 @@
             ffn[:, cols] = (mid[:, cols] * scale * ffng[0:1, cols]).astype(jnp.bfloat16)
         mid_out[...] = mid[pl.ds(pl.multiple_of(z * tok, tok), tok), :]
         for e in range(n_sp):
-            hit = jnp.where(meta[:, e : e + 1] == slot_id, 1.0, 0.0).astype(jnp.bfloat16)
+            hit = jnp.where(meta[e : e + 1, :] == slot_id, 1.0, 0.0).astype(jnp.bfloat16)
             for c in range(D // ct):
                 cols = slice(c * ct, (c + 1) * ct)
-                out_rows[e, :, cols] = split_dot(hit, ffn[:, cols], TN).astype(jnp.bfloat16)
+                out_rows[e, :, cols] = split_dot(hit, ffn[:, cols], NN).astype(jnp.bfloat16)
 
         for copy in meta_copies + res_copies + att_copies:
             copy.wait_send()
@@ -569,17 +715,20 @@
 
     dma = pltpu.SemaphoreType.DMA
     bf, f4 = jnp.bfloat16, jnp.float32
-    specs = [vmem()] * 9 + [pl.BlockSpec(memory_space=pl.ANY)] + [vmem()] * 6
+    specs = [vmem()] * 9 + [pl.BlockSpec(memory_space=pl.ANY)] + [vmem()] * 4
     return pl.pallas_call(
         kernel,
         out_shape=(
             jax.ShapeDtypeStruct((n_sp, rows, D), bf),
-            jax.ShapeDtypeStruct((n_sp, part, rows), bf),
+            jax.ShapeDtypeStruct((n_sp, rows, part), bf),
             jax.ShapeDtypeStruct((tok, D), f4),
         ),
         in_specs=specs,
         out_specs=(vmem(),) * 3,
         scratch_shapes=[
+            pltpu.VMEM((2, length, lanes), f4),
+            pltpu.VMEM((8, lanes), f4),
+            pltpu.VMEM((8, lanes), f4),
             pltpu.VMEM((heads, 2, length, 2 * lanes), bf),
             pltpu.VMEM((n_sp, bundle, lanes), bf),
             pltpu.VMEM((heads, length, lanes), f4),
@@ -590,7 +739,7 @@
             pltpu.VMEM((part, n_tp * lanes), bf),
             pltpu.VMEM(out_weight.shape, bf),
             pltpu.VMEM((n_z, tok, D), bf),
-            pltpu.VMEM((n_z, tok, lanes), f4),
+            pltpu.VMEM((n_z, 2 * named_rows, lanes), f4),
             pltpu.VMEM((part, D), f4),
             pltpu.VMEM((part, D), bf),
             dma((1,)),
@@ -610,30 +759,19 @@
         name="front",
     )(
         queries, latent, rot_key, lat_gain, key_up, value_up, q_gain, k_gain, out_gain,
-        out_weight, residual, ffn_gain, routes, weights, cosine, sine,
+        out_weight, residual, ffn_gain, routes, weights,
     )
-
-
-def packed_gain(gain, heads):
-    nope = jnp.tile(gain[:NOPE], 2)
-    rot = jnp.concatenate([jnp.tile(gain[NOPE:], heads), jnp.zeros((128 - heads * ROPE,))])
-    return jnp.concatenate([nope, rot])[None, :]
 
 
 def shards(
     queries, latent, rot_key, latent_gain, key_up, value_up, query_gain, key_gain, out_gain,
     out_weight, residual, ffn_gain, routes, route_weights, expert_gate, expert_up, expert_down,
 ):
-    length = queries.shape[0]
     heads = key_up.shape[1] // NOPE
     n_sp = lax.axis_size("sp")
     n_tp = lax.axis_size("tp")
     n_z = n_tp // 2
     width = heads * VH
-    first = lax.axis_index("sp") * length
-    positions = (first + jnp.arange(length, dtype=jnp.int32)).astype(jnp.float32)
-    inverse = rope_base ** (-jnp.arange(0, ROPE, 2, dtype=jnp.float32) / ROPE)
-    angles = positions[:, None] * jnp.tile(inverse, 128 // (ROPE // 2))[None, :]
     out_gain = out_gain.reshape(n_tp, 1, width)
     if width < 128:
         spare = 128 - width
@@ -644,19 +782,12 @@
             out_weight.reshape(n_tp, width, D), ((0, 0), (0, spare), (0, 0))
         ).reshape(n_tp * 128, D)
     outbound, mixer, middle = front(
-        queries, latent, rot_key, latent_gain[None, :], key_up, value_up,
-        packed_gain(query_gain, heads), packed_gain(key_gain, heads), out_gain, out_weight,
-        residual, ffn_gain[None, :], routes, route_weights, jnp.cos(angles), jnp.sin(angles),
-        n_sp, n_z, n_tp * width,
+        queries.T, latent, rot_key.T, latent_gain[None, :], key_up, value_up,
+        query_gain[None, :], key_gain[None, :], out_gain, out_weight,
+        residual, ffn_gain[None, :], routes.T, route_weights.T, n_sp, n_z, n_tp * width,
     )
-    rows = outbound.shape[1]
-    arrived = send_rows(outbound, n_sp, n_z)
-    row_block = arrived.reshape(2 * n_sp * rows, D)
-    gate_pre = jnp.dot(row_block, expert_gate[0], preferred_element_type=jnp.float32)
-    up_pre = jnp.dot(row_block, expert_up[0], preferred_element_type=jnp.float32)
-    hidden = (jax.nn.silu(gate_pre) * up_pre).astype(jnp.bfloat16)
-    return return_rows(
-        hidden.reshape(2, n_sp, rows, -1), expert_down[0], mixer, middle, n_sp, n_z
+    return experts(
+        outbound, mixer, middle, expert_gate[0], expert_up[0], expert_down[0], n_sp, n_z
     )
 
 

time: 143 us -> 116 us (0.81)
  local copies, waits for them, and re-layouts: 11.1 us -> 1.67 us
  Pallas kernels: 123 us -> 114 us
  matrix products: 6.25 us -> 0 us
  other arithmetic: 2.46 us -> 0 us
    dot_general x2 -> x0, matrix products: 6.25 us -> none  [the longest x1 3.89 us: shards(): jnp.dot(row_block, expert_gate[0], preferred_element_type=jnp.float32)]
    unnamed x11 -> x1, local copies, waits for them, and re-layouts: 7.83 us -> 1.67 us
    pallas_call x2 -> x1, Pallas kernels: 76.2 us -> 70 us  [experts(): pl.pallas_call(kernel, out_shape=jax.ShapeDtypeStruct((tok, D), bf), in_s...]
    pallas_call x1, Pallas kernels: 46.3 us -> 44 us  [front(): pl.pallas_call(kernel, out_shape=(jax.ShapeDtypeStruct((n_sp, rows, D), b...]
    sin x1 -> x0, other arithmetic: 1.79 us -> none  [shards(): jnp.sin(angles)]
    another operation x10 -> x0, local copies, waits for them, and re-layouts: 1.66 us -> none  [the longest x4 1.48 us: packed_gain(): nope = jnp.tile(gain[:NOPE], 2)]
    slice x2 -> x0, local copies, waits for them, and re-layouts: 1.54 us -> none  [packed_gain(): gain[NOPE:]]
where the time goes in v2:
time: 116 us
  Pallas kernels  114 us (98%)
  local copies, waits for them, and re-layouts  1.67 us (1%)
    pallas_call x1, Pallas kernels, experts(): pl.pallas_call(kernel, out_shape=jax.ShapeDtypeStruct((tok, D), bf), in_s...  70 us
    pallas_call x1, Pallas kernels, front(): pl.pallas_call(kernel, out_shape=(jax.ShapeDtypeStruct((n_sp, rows, D), b...  44 us

profile of v2, /device:TPU:0, one launch (start us, length us, event | category | flops | bytes accessed | tf_op | source)
XLA Modules:
  0.0 115.7 jit_solution(1226135394786341940)
XLA Ops:
  0.0 44.0 %front.1 = (bf16[4,144,2048]{2,1,0:T(8,128)(2,1)}, bf16[4,144,256]{2,1,0:T(8,128)(2,1)}, f32[64,2048]{1,0:T(8,128)}) custom-call(bf16[192,512]{1,0:T(8,128)(2,1)} %bitcast.15, bf16[512,512]{1,0:T(8,128)(2,1)} %lat_in.1, bf16[32,512]{1,0:T(8,128)(2,1)} %bitcast.16, f32[1,512]{1,0:T(1,128)} %bitcast.19, bf16[512,128]{1,0:T(8,128)(2,1)} %kup.1, ...), custom_call_target="tpu_custom_call" | custom-call | tf_op jit(solution)/shard_map/front/pallas_call | solution.py:719
  44.0 70.0 %experts.1 = bf16[64,2048]{1,0:T(8,128)(2,1)} custom-call(bf16[4,144,2048]{2,1,0:T(8,128)(2,1)} %get-tuple-element.8.x_in, bf16[4,144,256]{2,1,0:T(8,128)(2,1)} %get-tuple-element.9.mix_in, f32[64,2048]{1,0:T(8,128)} %get-tuple-element.10.mid_in, bf16[2048,256]{1,0:T(8,128)(2,1)} %bitcast.12, bf16[2048,256]{1,0:T(8,128)(2,1)} %bitcast.13, ...), custom_call_target="tpu_custom_call" | custom-call | tf_op jit(solution)/shard_map/experts/pallas_call | solution.py:312
  114.1 1.7 %copy.19 = bf16[64,2048]{1,0:T(8,128)(2,1)} copy(bf16[64,2048]{1,0:T(8,128)(2,1)} %experts.1) | data formatting | bytes 524288

commit v3 on v2

--- a/solution.py
+++ b/solution.py
@@ -86,11 +86,11 @@
 
 CHUNKS = 8
 PIECES = 3
-
-
-def experts(outbound, mixer, middle, gate, up, down, n_sp, n_z):
-    rows = outbound.shape[1]
-    tok = middle.shape[0]
+WIDE = 512
+LEAD = 3
+
+
+def expert_plan(rows, tok, gate, up, down, n_sp, n_z):
     width = D // CHUNKS
     hidden = gate.shape[1]
     shared = D // 4
@@ -98,20 +98,20 @@
     piece = half // PIECES
     phases = [[1, 2]] + [[k] for k in range(3, n_sp)] if n_sp > 2 else [[1]]
 
-    def kernel(
-        x_in, mix_in, mid_in, gate_hbm, up_hbm, down_hbm, o_ref,
-        gbuf, ubuf, dbuf, xbuf, hid, ybuf, pbuf, sbuf, rbuf, cbuf, fbuf,
-        w_sem, a_s, a_r, b_s, b_r, t_s, t_r, pa_s, pa_r, pb_s, pb_r, pt_s, pt_r, po_s, po_r,
-        y_s, y_r, sp_s, sp_r, z_s, z_r,
-    ):
-        place = Place(n_sp, n_z)
+    def loads_of(ins, scratch):
+        return [
+            pltpu.make_async_copy(src, dst, scratch[-9].at[i])
+            for i, (src, dst) in enumerate(zip(ins, scratch[:3]))
+        ]
+
+    def body(place, given, ins, o_ref, scratch):
+        x_in, mix_in, mid_in = given
+        (
+            gbuf, ubuf, dbuf, xbuf, hid, ybuf, pbuf, sbuf, rbuf, cbuf, fbuf,
+            w_sem, sent, a_r, b_r, t_r, p_r, y_r, sp_r, z_r,
+        ) = scratch
         core, z, me = place.core, place.z, place.sp
-        loads = []
-        for i, (src, dst) in enumerate(((gate_hbm, gbuf), (up_hbm, ubuf), (down_hbm, dbuf))):
-            load = pltpu.make_async_copy(src, dst, w_sem.at[i])
-            load.start()
-            loads.append(load)
-        place.barrier(True, True)
+        loads = loads_of(ins, scratch)
         side = lax.rem(z, 2)
         twin = place.z_id(z + 1 - 2 * side)
         partner = place.partner()
@@ -120,49 +120,44 @@
         def strip(which, p):
             return pl.ds(pl.multiple_of(shared + which * half + p * piece, 128), piece)
 
-        copies = []
-
-        def push(src, dst, send, recv, device):
-            copy = remote(src, dst, send, recv, device)
+        def push(src, dst, kind, recv, device):
+            copy = remote(src, dst, sent.at[kind], recv, device)
             copy.start()
-            copies.append(copy)
             return copy
 
-        own_in = push(
-            x_in.at[me], xbuf.at[core, me], po_s.at[0], po_r.at[0], partner
-        )
-        strips, shares, swaps, to_pair = {}, {}, {}, {k: [] for k in range(n_sp)}
+        push(x_in.at[me], xbuf.at[core, me], 3, p_r.at[0], partner)
+        strips, shares, swaps = {}, {}, {}
         for ks in phases:
             for p in range(PIECES):
                 for k in ks:
                     dst = flip(me, k)
                     cols = strip(side, p)
                     strips[k, p] = push(
-                        x_in.at[dst, :, cols], xbuf.at[core, me, :, cols],
-                        a_s.at[k, p], a_r.at[k, p], place.sp_id(dst),
+                        x_in.at[dst, :, cols], xbuf.at[core, me, :, cols], 0, a_r.at[k, p],
+                        place.sp_id(dst),
                     )
             for k in ks:
                 dst = flip(me, k)
                 shares[k] = push(
-                    x_in.at[dst, :, both], xbuf.at[core, me, :, both],
-                    b_s.at[k], b_r.at[k], place.sp_id(dst),
+                    x_in.at[dst, :, both], xbuf.at[core, me, :, both], 1, b_r.at[k],
+                    place.sp_id(dst),
                 )
 
         def forward_strip(k, p):
             block = xbuf.at[core, flip(me, k), :, strip(side, p)]
             strips[k, p].wait_recv()
-            swaps[k, p] = push(block, block, t_s.at[k, p], t_r.at[k, p], twin)
-            to_pair[k].append(push(block, block, pa_s.at[k, p], pa_r.at[k, p], partner))
+            swaps[k, p] = push(block, block, 2, t_r.at[k, p], twin)
+            push(block, block, 3, p_r.at[k], partner)
 
         def forward_share(k):
             block = xbuf.at[core, flip(me, k), :, both]
             shares[k].wait_recv()
-            to_pair[k].append(push(block, block, pb_s.at[k], pb_r.at[k], partner))
+            push(block, block, 3, p_r.at[k], partner)
 
         def forward_swap(k, p):
             block = xbuf.at[core, flip(me, k), :, strip(1 - side, p)]
             swaps[k, p].wait_recv()
-            to_pair[k].append(push(block, block, pt_s.at[k, p], pt_r.at[k, p], partner))
+            push(block, block, 3, p_r.at[k], partner)
 
         def expert(x_ref, h_ref):
             g = jnp.dot(x_ref[...], gbuf[...], preferred_element_type=jnp.float32)
@@ -172,19 +167,16 @@
         def column(q):
             return pl.ds(pl.multiple_of(q * width, width), width)
 
-        def pair_copy(k, q):
-            src = flip(me, k)
-            return remote(
-                ybuf.at[src, :, column(q)], pbuf.at[src, :, column(q)],
-                y_s.at[k, q], y_r.at[k, q], partner,
-            )
-
         def back_copy(k, q):
             src = flip(me, k)
             return remote(
-                sbuf.at[src, :, column(q)], rbuf.at[me, :, column(q)],
-                sp_s.at[k, q], sp_r.at[k, q], place.sp_id(src),
-            )
+                pbuf.at[src, :, column(q)], rbuf.at[me, :, column(q)],
+                sent.at[5], sp_r.at[k, q], place.sp_id(src),
+            )
+
+        def whole(k, buf, recv):
+            block = buf.at[flip(me, k)]
+            return remote(block, block, sent.at[4], recv.at[k], partner)
 
         def expert_own(k):
             src = flip(me, k)
@@ -192,40 +184,47 @@
 
         def expert_pair(k):
             src = flip(me, k)
+            whole(k, xbuf.at[1 - core], p_r).wait_recv()
+            expert(xbuf.at[1 - core, src], hid.at[1 - core, src])
+            for w in range(D // WIDE):
+                cols = slice(w * WIDE, (w + 1) * WIDE)
+                ybuf[src, :, cols] = jnp.dot(
+                    hid[1 - core, src], dbuf[:, cols], preferred_element_type=jnp.float32
+                ).astype(jnp.bfloat16)
+                remote(
+                    ybuf.at[src, :, cols], pbuf.at[src, :, cols], sent.at[4], y_r.at[k], partner
+                ).start()
+
+        def down_own(k):
+            src = flip(me, k)
+            for w in range(D // WIDE):
+                cols = slice(w * WIDE, (w + 1) * WIDE)
+                sbuf[src, :, cols] = jnp.dot(
+                    hid[core, src], dbuf[:, cols], preferred_element_type=jnp.float32
+                ).astype(jnp.bfloat16)
+
+        def settle(k, q):
+            src = flip(me, k)
+            total = sbuf[src, :, column(q)].astype(jnp.float32) + pbuf[
+                src, :, column(q)
+            ].astype(jnp.float32)
             if k == 0:
-                own_in.wait_recv()
-            for copy in to_pair[k]:
-                copy.wait_recv()
-            expert(xbuf.at[1 - core, src], hid.at[1 - core, src])
-
-            def body(q, carry):
-                ybuf[src, :, column(q)] = jnp.dot(
-                    hid[1 - core, src], dbuf[:, column(q)], preferred_element_type=jnp.float32
-                ).astype(jnp.bfloat16)
-                pair_copy(k, q).start()
-                return carry
-
-            lax.fori_loop(0, CHUNKS, body, 0)
-
-        def finish(ks):
+                rbuf[src, :, column(q)] = total.astype(jnp.bfloat16)
+            else:
+                pbuf[src, :, column(q)] = total.astype(jnp.bfloat16)
+                back_copy(k, q).start()
+
+        def finish(ks, first, last):
             def body(q, carry):
                 for k in ks:
-                    src = flip(me, k)
-                    own = jnp.dot(
-                        hid[core, src], dbuf[:, column(q)], preferred_element_type=jnp.float32
-                    )
-                    pair_copy(k, q).wait_recv()
-                    total = (own + pbuf[src, :, column(q)].astype(jnp.float32)).astype(
-                        jnp.bfloat16
-                    )
-                    if k == 0:
-                        rbuf[src, :, column(q)] = total
-                    else:
-                        sbuf[src, :, column(q)] = total
-                        back_copy(k, q).start()
+                    settle(k, q)
                 return carry
 
-            lax.fori_loop(0, CHUNKS, body, 0)
+            lax.fori_loop(first, last, body, 0)
+
+        def take_pair(ks):
+            for k in ks:
+                whole(k, pbuf, y_r).wait_recv()
 
         def arrivals(ks):
             steps = []
@@ -242,29 +241,46 @@
         loads[2].wait()
         expert_pair(0)
         waiting.pop(0)()
-        finish([0])
+        down_own(0)
+        take_pair([0])
+        finish([0], 0, CHUNKS)
         for index, ks in enumerate(phases):
             while waiting:
                 waiting.pop(0)()
+            waiting = arrivals(phases[index + 1]) if index + 1 < len(phases) else []
             for p in range(PIECES):
                 for k in ks:
                     forward_swap(k, p)
-            waiting = arrivals(phases[index + 1]) if index + 1 < len(phases) else []
+                if waiting and p < 2:
+                    waiting.pop(0)()
             for k in ks:
                 expert_own(k)
-            if waiting:
-                waiting.pop(0)()
+            for k in ks:
+                down_own(k)
             for k in ks:
                 expert_pair(k)
                 if waiting:
                     waiting.pop(0)()
-            finish(ks)
+            take_pair(ks)
+            if index + 1 == len(phases) and index:
+
+                def last(q, carry, ks=ks):
+                    for k in ks:
+                        settle(k, q)
+                    for k in phases[-2]:
+                        settle(k, q + LEAD)
+                    return carry
+
+                lax.fori_loop(0, CHUNKS - LEAD, last, 0)
+                finish(ks, CHUNKS - LEAD, CHUNKS)
+            else:
+                finish(ks, 0, LEAD if index + 2 == len(phases) else CHUNKS)
 
         def z_copy(q, step):
             dst = place.z_peer(step)
             return remote(
                 cbuf.at[dst, :, column(q)], fbuf.at[z, :, column(q)],
-                z_s.at[q, step], z_r.at[q, step], place.z_id(dst),
+                sent.at[6], z_r.at[q, step], place.z_id(dst),
             )
 
         def combine(q, carry):
@@ -291,30 +307,25 @@
 
         lax.fori_loop(0, CHUNKS, close, 0)
 
-        def drain(q, carry):
-            for k in range(n_sp):
-                pair_copy(k, q).wait_send()
-            for k in range(1, n_sp):
-                back_copy(k, q).wait_send()
-            for step in range(1, n_z):
-                z_copy(q, step).wait_send()
-            return carry
-
-        for copy in copies:
-            copy.wait_send()
-        lax.fori_loop(0, CHUNKS, drain, 0)
+        others = pl.ds(0, n_sp - 1)
+        strip_bytes = xbuf.at[0, others, :, pl.ds(shared, half)]
+        for kind, block in enumerate(
+            (
+                strip_bytes, xbuf.at[0, others, :, both], strip_bytes, ybuf, ybuf,
+                ybuf.at[others], fbuf.at[pl.ds(0, n_z - 1)],
+            )
+        ):
+            remote(block, block, sent.at[kind], z_r.at[0, 0], partner).wait_send()
 
     dma = pltpu.SemaphoreType.DMA
     bf = jnp.bfloat16
     block = pltpu.VMEM((n_sp, rows, D), bf)
     zblock = pltpu.VMEM((n_z, tok, D), bf)
-    any_spec = pl.BlockSpec(memory_space=pl.ANY)
-    return pl.pallas_call(
-        kernel,
-        out_shape=jax.ShapeDtypeStruct((tok, D), bf),
-        in_specs=[vmem()] * 3 + [any_spec] * 3,
-        out_specs=vmem(),
-        scratch_shapes=[
+    return dict(
+        body=body,
+        loads=loads_of,
+        ins=(gate, up, down),
+        scratch=[
             pltpu.VMEM(gate.shape, bf),
             pltpu.VMEM(up.shape, bf),
             pltpu.VMEM(down.shape, bf),
@@ -322,20 +333,93 @@
             pltpu.VMEM((2, n_sp, rows, hidden), bf),
             block, block, block, block, zblock, zblock,
             dma((3,)),
-        ]
-        + [dma((n_sp, PIECES))] * 2
-        + [dma((n_sp,))] * 2
-        + [dma((n_sp, PIECES))] * 4
-        + [dma((n_sp,))] * 2
-        + [dma((n_sp, PIECES))] * 2
-        + [dma((1,))] * 2
-        + [dma((n_sp, CHUNKS))] * 4
-        + [dma((CHUNKS, n_z))] * 2,
-        compiler_params=pltpu.CompilerParams(
-            collective_id=1, has_side_effects=True, vmem_limit_bytes=62 << 20
-        ),
+            dma((7,)),
+            dma((n_sp, PIECES)),
+            dma((n_sp,)),
+            dma((n_sp, PIECES)),
+            dma((n_sp,)),
+            dma((n_sp,)),
+            dma((n_sp, CHUNKS)),
+            dma((CHUNKS, n_z)),
+        ],
+    )
+
+
+VMEM_ROOM = 63 << 20
+
+
+def run_plans(first, second, tok, n_sp, n_z):
+    hbm = pl.BlockSpec(memory_space=pl.ANY)
+    out_shape = jax.ShapeDtypeStruct((tok, D), jnp.bfloat16)
+    n_ins, n_first, n_given = len(first["ins"]), len(first["scratch"]), len(first["outs"])
+    given = [pltpu.VMEM(shape, dtype) for shape, dtype in first["outs"]]
+    sizes = first["scratch"] + second["scratch"] + given
+    need = sum(
+        int(np.prod(one.inner_aval.shape)) * one.inner_aval.dtype.itemsize
+        for one in sizes
+        if "vmem" in str(one.memory_space)
+    )
+
+    def params(number, room):
+        return pltpu.CompilerParams(
+            collective_id=number, has_side_effects=True, vmem_limit_bytes=room
+        )
+
+    def merged(*refs):
+        place = Place(n_sp, n_z)
+        ins, weights, refs = refs[:n_ins], refs[n_ins : n_ins + 3], refs[n_ins + 3 :]
+        o_ref, held, refs = refs[0], refs[1 : 1 + n_given], refs[1 + n_given :]
+        drain = first["body"](place, ins, held, refs[:n_first], second["loads"](weights, refs[n_first:]))
+        second["body"](place, held, weights, o_ref, refs[n_first:])
+        drain()
+
+    if need < 52 << 20:
+        return pl.pallas_call(
+            merged,
+            out_shape=out_shape,
+            in_specs=first["in_specs"] + [hbm] * 3,
+            out_specs=vmem(),
+            scratch_shapes=given + first["scratch"] + second["scratch"],
+            compiler_params=params(0, VMEM_ROOM),
+            name="layer",
+        )(*first["ins"], *second["ins"])
+
+    def head(*refs):
+        place = Place(n_sp, n_z)
+        ins, outs = refs[:n_ins], refs[n_ins : n_ins + n_given]
+        first["body"](place, ins, outs, refs[n_ins + n_given :], [])()
+
+    def tail(*refs):
+        place = Place(n_sp, n_z)
+        scratch = refs[n_given + 4 :]
+        for load in second["loads"](refs[n_given : n_given + 3], scratch):
+            load.start()
+        place.barrier(True, True)
+        second["body"](
+            place, refs[:n_given], refs[n_given : n_given + 3], refs[n_given + 3], scratch
+        )
+
+    held = pl.pallas_call(
+        head,
+        out_shape=tuple(jax.ShapeDtypeStruct(*one) for one in first["outs"]),
+        in_specs=first["in_specs"],
+        out_specs=(vmem(),) * n_given,
+        scratch_shapes=first["scratch"],
+        compiler_params=params(0, VMEM_ROOM),
+        name="front",
+    )(*first["ins"])
+    return pl.pallas_call(
+        tail,
+        out_shape=out_shape,
+        in_specs=[vmem()] * n_given + [hbm] * 3,
+        out_specs=vmem(),
+        scratch_shapes=second["scratch"],
+        compiler_params=params(1, VMEM_ROOM),
         name="experts",
-    )(outbound, mixer, middle, gate, up, down)
+    )(*held, *second["ins"])
+
+
+RES_PARTS = 4
 
 
 def split_dot(a, b, dims):
@@ -347,7 +431,7 @@
 TN = ((0,), (0,))
 
 
-def front(
+def front_plan(
     queries, latent, rot_key, lat_gain, key_up, value_up, q_gain, k_gain, out_gain,
     out_weight, residual, ffn_gain, routes, weights, n_sp, n_z, width,
 ):
@@ -368,16 +452,18 @@
     freqs = ROPE // 2
     inverse = np.float32(rope_base) ** (-np.arange(0, ROPE, 2, dtype=np.float32) / np.float32(ROPE))
 
-    def kernel(
-        q_in, lat_in, rot_in, latg, kup, vup, qg, kg, outg, w_hbm, res_in, ffng, routes_in,
-        weights_in, out_rows, mixer, mid_out,
-        table, gains, tokens, qbuf, kv, peak, total, acc, att, gath, normed, wbuf, resbuf, metabuf, mid, ffn,
-        w_sem, local_sem, kv_s, kv_r, res_s, res_r, meta_s, meta_r, att_s, att_r,
-    ):
-        place = Place(n_sp, n_z)
+    def body(place, ins, outs, scratch, more_loads):
+        (
+            q_hbm, lat_hbm, rot_in, latg, kup_hbm, vup_hbm, qg, kg, outg, w_hbm, res_hbm, ffng,
+            routes_in, weights_in,
+        ) = ins
+        out_rows, mixer, mid_out = outs
+        (
+            q_in, lat_in, kup, vup, table, gains, tokens, qbuf, kv, peak, total, acc, att, gath,
+            normed, wbuf, resbuf, metabuf, mid, ffn, load_sem, sent, kv_s, kv_r, res_r, meta_r,
+            att_r,
+        ) = scratch
         sp, core, z, tp = place.sp, place.core, place.z, place.tp
-        load_w = pltpu.make_async_copy(w_hbm, wbuf, w_sem.at[0])
-        load_w.start()
         sem = pltpu.get_barrier_semaphore()
         for step in range(1, n_tp):
             pl.semaphore_signal(
@@ -387,6 +473,18 @@
             pl.semaphore_signal(
                 sem, inc=1, device_id=place.sp_id(place.sp_peer(step)), device_id_type=MESH_ID
             )
+        loads = []
+        for i, (src, dst) in enumerate(
+            (
+                (lat_hbm, lat_in), (kup_hbm, kup), (vup_hbm, vup), (q_hbm, q_in),
+                (res_hbm, resbuf.at[z]), (w_hbm, wbuf),
+            )
+        ):
+            load = pltpu.make_async_copy(src, dst, load_sem.at[i])
+            load.start()
+            loads.append(load)
+        for load in more_loads:
+            load.start()
 
         tokens[0:1, :] = jnp.full((1, lanes), -1.0, jnp.float32)
         tokens[1:2, :] = jnp.full((1, lanes), -1.0, jnp.float32)
@@ -413,10 +511,12 @@
                 metabuf[z, :named_rows] = pltpu.roll(slot, turn_by * tok, 1) if turn_by else slot
                 metabuf[z, named_rows:] = pltpu.roll(share, turn_by * tok, 1) if turn_by else share
 
-        freq_id = lax.broadcasted_iota(jnp.int32, (freqs, pt), 0)
-        freq = jnp.zeros((freqs, pt), jnp.float32)
+        freq_id = lax.broadcasted_iota(jnp.int32, (freqs, length), 0)
+        freq = jnp.zeros((freqs, length), jnp.float32)
         for i in range(freqs):
             freq = jnp.where(freq_id == i, float(inverse[i]), freq)
+        where = lax.broadcasted_iota(jnp.int32, (freqs, length), 1) + sp * length
+        angle = where.astype(jnp.float32) * freq
         spread_by = jnp.where(
             lax.broadcasted_iota(jnp.int32, (freqs, lanes), 1) % freqs
             == lax.broadcasted_iota(jnp.int32, (freqs, lanes), 0),
@@ -424,18 +524,11 @@
             0.0,
         )
 
-        def make_table(i, carry):
-            where = lax.broadcasted_iota(jnp.int32, (freqs, pt), 1) + (sp * length + i * pt)
-            angle = where.astype(jnp.float32) * freq
-            at = pl.ds(pl.multiple_of(i * pt, pt), pt)
-            for which, values in enumerate((jnp.cos(angle), jnp.sin(angle))):
-                table[which, at, :] = lax.dot_general(
-                    values, spread_by, (TN, ((), ())), precision=lax.Precision.HIGHEST,
-                    preferred_element_type=jnp.float32,
-                )
-            return carry
-
-        lax.fori_loop(0, length // pt, make_table, 0)
+        for which, values in enumerate((jnp.cos(angle), jnp.sin(angle))):
+            table[which] = lax.dot_general(
+                values, spread_by, (TN, ((), ())), precision=lax.Precision.HIGHEST,
+                preferred_element_type=jnp.float32,
+            )
         for i, gain in enumerate((qg, kg)):
             gains[4 + i : 5 + i, :] = jnp.zeros((1, lanes), jnp.float32)
             gains[4 + i : 5 + i, :QK] = gain[...]
@@ -452,28 +545,46 @@
         (q_nope_gain, q_rot_gain), (k_nope_gain, k_rot_gain) = packed
 
         pl.semaphore_wait(sem, n_tp - 1 + n_sp - 1)
-        sends = []
-
-        def push(src, dst, send, recv, device):
-            copy = remote(src, dst, send, recv, device)
+        def push(src, dst, kind, recv, device):
+            copy = remote(src, dst, sent.at[kind], recv, device)
             copy.start()
             return copy
 
-        res_copies, meta_copies = [], []
+        parts = [slice(i * D // RES_PARTS, (i + 1) * D // RES_PARTS) for i in range(RES_PARTS)]
+
+        def res_copy(src, i, to, src_ref=None):
+            block = resbuf.at[src, :, parts[i]]
+            from_ref = block if src_ref is None else src_ref.at[:, parts[i]]
+            return remote(
+                from_ref, block, sent.at[0], res_r.at[src, i], place.z_id(to)
+            )
+
+        for i in range(RES_PARTS):
+            for away in (2, -2, 1, -1):
+                to = z + away
+
+                @pl.when((to >= 0) & (to < n_z))
+                def _(to=to, i=i):
+                    res_copy(z, i, to, res_hbm).start()
+
         for step in range(1, n_z):
             to = place.z_id(place.z_peer(step))
-            meta_copies.append(
-                push(metabuf.at[z], metabuf.at[z], meta_s.at[step], meta_r.at[step], to)
-            )
-        for step in range(1, n_z):
-            to = place.z_id(place.z_peer(step))
-            res_copies.append(push(res_in, resbuf.at[z], res_s.at[step], res_r.at[step], to))
-        local = pltpu.make_async_copy(res_in, resbuf.at[z], local_sem.at[0])
-        local.start()
+            push(metabuf.at[z], metabuf.at[z], 1, meta_r.at[z], to)
+
+        def pass_on(away, i):
+            for sign in (1, -1):
+                src, to = z - sign * away, z + sign
+
+                @pl.when((src >= 0) & (src < n_z) & (to >= 0) & (to < n_z))
+                def _(src=src, to=to):
+                    res_copy(src, i, z).wait_recv()
+                    res_copy(src, i, to).start()
 
         lane = lax.broadcasted_iota(jnp.int32, (1, lanes), 1)
         low = lane % ROPE < ROPE // 2
         mine = kv.at[sp]
+        for load in loads[:3]:
+            load.wait()
 
         def turn(values, cos, sin):
             return (
@@ -535,7 +646,7 @@
 
             @pl.when(dst < n_sp)
             def _(dst=dst):
-                push(mine, mine, kv_s.at[dst], kv_r.at[sp], place.sp_id(dst))
+                remote(mine, mine, kv_s.at[dst], kv_r.at[sp], place.sp_id(dst)).start()
 
         wide = 2 * lanes
         src_id = lax.broadcasted_iota(jnp.int32, (heads * QK, wide), 0)
@@ -548,6 +659,8 @@
                 (entry >= NOPE) & (entry < QK) & (dst_id == lanes + h * ROPE + entry - NOPE)
             )
             pickers.append(jnp.where(nope_hit | rot_hit, 1.0, 0.0).astype(jnp.bfloat16))
+
+        loads[3].wait()
 
         def make_queries(i, carry):
             at = pl.ds(pl.multiple_of(i * pt, pt), pt)
@@ -626,7 +739,16 @@
 
             return carry
 
-        lax.fori_loop(1, n_sp, visit, 0)
+        hops = [(away, i) for away in range(2, n_z - 1) for i in range(RES_PARTS)]
+        head = RES_PARTS // 2
+        for away, i in hops[:head]:
+            pass_on(away, i)
+        lax.fori_loop(1, 2, visit, 0)
+        for away, i in hops[head:RES_PARTS]:
+            pass_on(away, i)
+        lax.fori_loop(2, n_sp, visit, 0)
+        for away, i in hops[RES_PARTS:]:
+            pass_on(away, i)
 
         for block in range(n_tp):
             at = pl.ds(block * tok, tok)
@@ -636,23 +758,16 @@
             att[block % 2, (block // 2) * tok : (block // 2 + 1) * tok, :] = (
                 acc[at, :] / bottom
             ).astype(jnp.bfloat16)
-        att_copies = []
-        for step in range(1, n_tp):
+        for step in range(n_tp - 1, 0, -1):
             dst = lax.rem(tp + step, n_tp)
-            att_copies.append(
-                push(
-                    att.at[lax.rem(dst, 2)],
-                    gath.at[tp],
-                    att_s.at[step],
-                    att_r.at[step],
-                    (sp, dst),
-                )
-            )
-        own = pltpu.make_async_copy(att.at[core], gath.at[tp], local_sem.at[1])
+            push(att.at[lax.rem(dst, 2)], gath.at[tp], 2, att_r.at[tp], (sp, dst))
+        own = pltpu.make_async_copy(att.at[core], gath.at[tp], load_sem.at[6])
         own.start()
 
-        for copy in meta_copies:
-            copy.wait_recv()
+        partner = place.partner()
+        for step in range(1, n_z):
+            block = metabuf.at[place.z_peer(step)]
+            remote(block, block, sent.at[1], meta_r.at[place.z_peer(step)], partner).wait_recv()
         pieces = []
         for first in range(0, n_z, per):
             piece = metabuf[first]
@@ -666,14 +781,22 @@
             mixer[e] = jnp.where(
                 hit, meta[named_rows + e : named_rows + e + 1, :], 0.0
             ).astype(jnp.bfloat16)
-        for copy in res_copies:
-            copy.wait_recv()
-        local.wait()
-        load_w.wait()
+        for i in range(RES_PARTS):
+            for src in range(n_z):
+                away = z - src
+                passed = ((away >= 2) & (z + 1 < n_z)) | ((away <= -2) & (z > 0))
+
+                @pl.when((away != 0) & jnp.logical_not(passed))
+                def _(src=src, i=i):
+                    res_copy(src, i, z).wait_recv()
+
+        for load in loads[4:]:
+            load.wait()
         own.wait()
-        for copy in att_copies:
-            copy.wait_recv()
-
+        for step in range(1, n_tp):
+            src = lax.rem(tp + step, n_tp)
+            block = gath.at[src]
+            remote(block, block, sent.at[2], att_r.at[src], partner).wait_recv()
         square = None
         for t in range(n_tp):
             block = gath[t].astype(jnp.float32)
@@ -704,28 +827,58 @@
                 cols = slice(c * ct, (c + 1) * ct)
                 out_rows[e, :, cols] = split_dot(hit, ffn[:, cols], NN).astype(jnp.bfloat16)
 
-        for copy in meta_copies + res_copies + att_copies:
-            copy.wait_send()
-        for step in range(1, n_sp):
-            dst = sp + n_sp - step
-
-            @pl.when(dst < n_sp)
-            def _(dst=dst):
-                remote(mine, mine, kv_s.at[dst], kv_r.at[sp], place.sp_id(dst)).wait_send()
+        def drain():
+            for i in range(RES_PARTS):
+                block = resbuf.at[0, :, parts[i]]
+                one = remote(block, block, sent.at[0], res_r.at[0, 0], partner)
+                for away in (2, -2, 1, -1):
+
+                    @pl.when((z + away >= 0) & (z + away < n_z))
+                    def _(one=one):
+                        one.wait_send()
+
+            for away, i in hops:
+                block = resbuf.at[0, :, parts[i]]
+                one = remote(block, block, sent.at[0], res_r.at[0, 0], partner)
+                for sign in (1, -1):
+                    src, to = z - sign * away, z + sign
+
+                    @pl.when((src >= 0) & (src < n_z) & (to >= 0) & (to < n_z))
+                    def _(one=one):
+                        one.wait_send()
+
+            block = metabuf.at[pl.ds(0, n_z - 1)]
+            remote(block, block, sent.at[1], meta_r.at[0], partner).wait_send()
+            block = gath.at[pl.ds(0, n_tp - 1)]
+            remote(block, block, sent.at[2], att_r.at[0], partner).wait_send()
+            for step in range(1, n_sp):
+                dst = sp + n_sp - step
+
+                @pl.when(dst < n_sp)
+                def _(dst=dst):
+                    remote(mine, mine, kv_s.at[dst], kv_r.at[sp], place.sp_id(dst)).wait_send()
+
+        return drain
 
     dma = pltpu.SemaphoreType.DMA
     bf, f4 = jnp.bfloat16, jnp.float32
-    specs = [vmem()] * 9 + [pl.BlockSpec(memory_space=pl.ANY)] + [vmem()] * 4
-    return pl.pallas_call(
-        kernel,
-        out_shape=(
-            jax.ShapeDtypeStruct((n_sp, rows, D), bf),
-            jax.ShapeDtypeStruct((n_sp, rows, part), bf),
-            jax.ShapeDtypeStruct((tok, D), f4),
+    hbm = pl.BlockSpec(memory_space=pl.ANY)
+    return dict(
+        body=body,
+        ins=(
+            queries, latent, rot_key, lat_gain, key_up, value_up, q_gain, k_gain, out_gain,
+            out_weight, residual, ffn_gain, routes, weights,
         ),
-        in_specs=specs,
-        out_specs=(vmem(),) * 3,
-        scratch_shapes=[
+        in_specs=[
+            hbm, hbm, vmem(), vmem(), hbm, hbm, vmem(), vmem(), vmem(), hbm, hbm, vmem(),
+            vmem(), vmem(),
+        ],
+        outs=[((n_sp, rows, D), bf), ((n_sp, rows, part), bf), ((tok, D), f4)],
+        scratch=[
+            pltpu.VMEM(queries.shape, bf),
+            pltpu.VMEM(latent.shape, bf),
+            pltpu.VMEM(key_up.shape, bf),
+            pltpu.VMEM(value_up.shape, bf),
             pltpu.VMEM((2, length, lanes), f4),
             pltpu.VMEM((8, lanes), f4),
             pltpu.VMEM((8, lanes), f4),
@@ -742,24 +895,14 @@
             pltpu.VMEM((n_z, 2 * named_rows, lanes), f4),
             pltpu.VMEM((part, D), f4),
             pltpu.VMEM((part, D), bf),
-            dma((1,)),
-            dma((2,)),
+            dma((7,)),
+            dma((3,)),
             dma((n_sp,)),
             dma((n_sp,)),
-            dma((n_z,)),
-            dma((n_z,)),
-            dma((n_z,)),
+            dma((n_z, RES_PARTS)),
             dma((n_z,)),
             dma((n_tp,)),
-            dma((n_tp,)),
         ],
-        compiler_params=pltpu.CompilerParams(
-            collective_id=0, has_side_effects=True, vmem_limit_bytes=60 << 20
-        ),
-        name="front",
-    )(
-        queries, latent, rot_key, lat_gain, key_up, value_up, q_gain, k_gain, out_gain,
-        out_weight, residual, ffn_gain, routes, weights,
     )
 
 
@@ -781,14 +924,16 @@
         out_weight = jnp.pad(
             out_weight.reshape(n_tp, width, D), ((0, 0), (0, spare), (0, 0))
         ).reshape(n_tp * 128, D)
-    outbound, mixer, middle = front(
+    first = front_plan(
         queries.T, latent, rot_key.T, latent_gain[None, :], key_up, value_up,
         query_gain[None, :], key_gain[None, :], out_gain, out_weight,
         residual, ffn_gain[None, :], routes.T, route_weights.T, n_sp, n_z, n_tp * width,
     )
-    return experts(
-        outbound, mixer, middle, expert_gate[0], expert_up[0], expert_down[0], n_sp, n_z
+    cap = max(2, 9 * residual.shape[0] * TOPK // (8 * n_sp))
+    second = expert_plan(
+        n_z * cap, residual.shape[0], expert_gate[0], expert_up[0], expert_down[0], n_sp, n_z
     )
+    return run_plans(first, second, residual.shape[0], n_sp, n_z)
 
 
 def solution(mesh):

time: 116 us -> 104 us (0.90)
  the two profiles are of different devices: /device:TPU:0 before, /device:TPU:4 now
where the time goes in v3:
time: 104 us
  Pallas kernels  102 us (98%)
  local copies, waits for them, and re-layouts  1.67 us (2%)
    pallas_call x1, Pallas kernels, run_plans(): pl.pallas_call(merged, out_shape=out_shape, in_specs=first['in_specs'] +...  102 us

profile of v3, /device:TPU:4, one launch (start us, length us, event | category | flops | bytes accessed | tf_op | source)
XLA Modules:
  0.0 104.0 jit_solution(17439977447226954978)
XLA Ops:
  0.0 102.3 %layer.1 = bf16[64,2048]{1,0:T(8,128)(2,1)} custom-call(bf16[192,512]{1,0:T(8,128)(2,1)} %bitcast.15, bf16[512,512]{1,0:T(8,128)(2,1)} %refs_1_.1, bf16[32,512]{1,0:T(8,128)(2,1)} %bitcast.16, f32[1,512]{1,0:T(1,128)} %bitcast.19, bf16[512,128]{1,0:T(8,128)(2,1)} %refs_4_.1, bf16[512,128]{1,0:T(8,128)(2,1)} %refs_5_.1, f32[1,96]{1,0:T(1,128)} %bitcast.22, ...), custom_call_target="tpu_custom_call" | custom-call | tf_op jit(solution)/shard_map/layer/pallas_call | solution.py:377
  102.4 1.7 %copy.19 = bf16[64,2048]{1,0:T(8,128)(2,1)} copy(bf16[64,2048]{1,0:T(8,128)(2,1)} %layer.1) | data formatting | bytes 524288

commit v4 on v3

--- a/solution.py
+++ b/solution.py
@@ -85,79 +85,91 @@
 
 
 CHUNKS = 8
-PIECES = 3
+PIECES = 4
 WIDE = 512
-LEAD = 3
+LEAD = 5
+LAG = 2
 
 
 def expert_plan(rows, tok, gate, up, down, n_sp, n_z):
     width = D // CHUNKS
     hidden = gate.shape[1]
-    shared = D // 4
-    half = (D - shared) // 2
-    piece = half // PIECES
+    quarter = D // 4
     phases = [[1, 2]] + [[k] for k in range(3, n_sp)] if n_sp > 2 else [[1]]
 
-    def loads_of(ins, scratch):
+    def weight_refs(place, ins, scratch):
+        own = pl.ds(pl.multiple_of(place.core * hidden, 128), hidden)
+        gbuf, ubuf, dbuf = scratch[:3]
+        return list(zip(ins, (gbuf.at[:, own], ubuf.at[:, own], dbuf.at[own, :])))
+
+    def loads_of(place, ins, scratch):
         return [
-            pltpu.make_async_copy(src, dst, scratch[-9].at[i])
-            for i, (src, dst) in enumerate(zip(ins, scratch[:3]))
+            pltpu.make_async_copy(src, dst, scratch[-7].at[i])
+            for i, (src, dst) in enumerate(weight_refs(place, ins, scratch))
+        ]
+
+    def shares_of(place, ins, scratch):
+        return [
+            remote(src, dst, scratch[-7].at[3 + i], scratch[-7].at[6 + i], place.partner())
+            for i, (src, dst) in enumerate(weight_refs(place, ins, scratch))
         ]
 
     def body(place, given, ins, o_ref, scratch):
         x_in, mix_in, mid_in = given
         (
-            gbuf, ubuf, dbuf, xbuf, hid, ybuf, pbuf, sbuf, rbuf, cbuf, fbuf,
-            w_sem, sent, a_r, b_r, t_r, p_r, y_r, sp_r, z_r,
+            gbuf, ubuf, dbuf, xbuf, hid, sbuf, rbuf, cbuf, fbuf,
+            w_sem, sent, a_r, b_r, t_r, sp_r, z_r,
         ) = scratch
         core, z, me = place.core, place.z, place.sp
-        loads = loads_of(ins, scratch)
+        loads = loads_of(place, ins, scratch)
+        traded = shares_of(place, ins, scratch)
         side = lax.rem(z, 2)
         twin = place.z_id(z + 1 - 2 * side)
-        partner = place.partner()
-        both = pl.ds(0, shared)
-
-        def strip(which, p):
-            return pl.ds(pl.multiple_of(shared + which * half + p * piece, 128), piece)
+        final = phases[-1] if n_sp > 2 else []
+
+        def share(k):
+            return 0 if k in final else 2 * quarter
+
+        both = [pl.ds(i * quarter, quarter) for i in range(2)]
+
+        def strip(which, k, p):
+            half = (D - share(k)) // 2
+            piece = half // PIECES
+            return pl.ds(pl.multiple_of(share(k) + which * half + p * piece, 128), piece)
 
         def push(src, dst, kind, recv, device):
             copy = remote(src, dst, sent.at[kind], recv, device)
             copy.start()
             return copy
 
-        push(x_in.at[me], xbuf.at[core, me], 3, p_r.at[0], partner)
         strips, shares, swaps = {}, {}, {}
-        for ks in phases:
-            for p in range(PIECES):
-                for k in ks:
-                    dst = flip(me, k)
-                    cols = strip(side, p)
-                    strips[k, p] = push(
-                        x_in.at[dst, :, cols], xbuf.at[core, me, :, cols], 0, a_r.at[k, p],
-                        place.sp_id(dst),
-                    )
-            for k in ks:
-                dst = flip(me, k)
-                shares[k] = push(
-                    x_in.at[dst, :, both], xbuf.at[core, me, :, both], 1, b_r.at[k],
-                    place.sp_id(dst),
-                )
+        order = [(k, p) for ks in phases for p in range(PIECES) for k in ks]
+        halves = [(k, i) for ks in phases for i in range(2) for k in ks if k not in final]
+
+        def push_strip(k, p):
+            dst = flip(me, k)
+            cols = strip(side, k, p)
+            strips[k, p] = push(
+                x_in.at[dst, :, cols], xbuf.at[me, :, cols], 0, a_r.at[k, p], place.sp_id(dst)
+            )
+
+        near = [one for one in order if one[0] not in final]
+        far = [one for one in order if one[0] in final]
+        for k, p in near:
+            push_strip(k, p)
+        for k, i in halves:
+            dst = flip(me, k)
+            shares[k, i] = push(
+                x_in.at[dst, :, both[i]], xbuf.at[me, :, both[i]], 1, b_r.at[k, i],
+                place.sp_id(dst),
+            )
+        for k, p in far:
+            push_strip(k, p)
 
         def forward_strip(k, p):
-            block = xbuf.at[core, flip(me, k), :, strip(side, p)]
+            block = xbuf.at[flip(me, k), :, strip(side, k, p)]
             strips[k, p].wait_recv()
             swaps[k, p] = push(block, block, 2, t_r.at[k, p], twin)
-            push(block, block, 3, p_r.at[k], partner)
-
-        def forward_share(k):
-            block = xbuf.at[core, flip(me, k), :, both]
-            shares[k].wait_recv()
-            push(block, block, 3, p_r.at[k], partner)
-
-        def forward_swap(k, p):
-            block = xbuf.at[core, flip(me, k), :, strip(1 - side, p)]
-            swaps[k, p].wait_recv()
-            push(block, block, 3, p_r.at[k], partner)
 
         def expert(x_ref, h_ref):
             g = jnp.dot(x_ref[...], gbuf[...], preferred_element_type=jnp.float32)
@@ -170,120 +182,87 @@
         def back_copy(k, q):
             src = flip(me, k)
             return remote(
-                pbuf.at[src, :, column(q)], rbuf.at[me, :, column(q)],
-                sent.at[5], sp_r.at[k, q], place.sp_id(src),
-            )
-
-        def whole(k, buf, recv):
-            block = buf.at[flip(me, k)]
-            return remote(block, block, sent.at[4], recv.at[k], partner)
-
-        def expert_own(k):
+                sbuf.at[src, :, column(q)], rbuf.at[me, :, column(q)],
+                sent.at[3], sp_r.at[k, q], place.sp_id(src),
+            )
+
+        def serve(k):
             src = flip(me, k)
-            expert(x_in.at[me] if k == 0 else xbuf.at[core, src], hid.at[core, src])
-
-        def expert_pair(k):
-            src = flip(me, k)
-            whole(k, xbuf.at[1 - core], p_r).wait_recv()
-            expert(xbuf.at[1 - core, src], hid.at[1 - core, src])
+            expert(x_in.at[me] if k == 0 else xbuf.at[src], hid.at[0])
             for w in range(D // WIDE):
                 cols = slice(w * WIDE, (w + 1) * WIDE)
-                ybuf[src, :, cols] = jnp.dot(
-                    hid[1 - core, src], dbuf[:, cols], preferred_element_type=jnp.float32
+                total = jnp.dot(
+                    hid[0], dbuf[:, cols], preferred_element_type=jnp.float32
                 ).astype(jnp.bfloat16)
-                remote(
-                    ybuf.at[src, :, cols], pbuf.at[src, :, cols], sent.at[4], y_r.at[k], partner
-                ).start()
-
-        def down_own(k):
-            src = flip(me, k)
-            for w in range(D // WIDE):
-                cols = slice(w * WIDE, (w + 1) * WIDE)
-                sbuf[src, :, cols] = jnp.dot(
-                    hid[core, src], dbuf[:, cols], preferred_element_type=jnp.float32
-                ).astype(jnp.bfloat16)
-
-        def settle(k, q):
-            src = flip(me, k)
-            total = sbuf[src, :, column(q)].astype(jnp.float32) + pbuf[
-                src, :, column(q)
-            ].astype(jnp.float32)
-            if k == 0:
-                rbuf[src, :, column(q)] = total.astype(jnp.bfloat16)
-            else:
-                pbuf[src, :, column(q)] = total.astype(jnp.bfloat16)
-                back_copy(k, q).start()
-
-        def finish(ks, first, last):
+                if k == 0:
+                    rbuf[src, :, cols] = total
+                else:
+                    sbuf[src, :, cols] = total
+
+        def reply(ks, first, last):
             def body(q, carry):
                 for k in ks:
-                    settle(k, q)
+                    back_copy(k, q).start()
                 return carry
 
             lax.fori_loop(first, last, body, 0)
 
-        def take_pair(ks):
-            for k in ks:
-                whole(k, pbuf, y_r).wait_recv()
-
-        def arrivals(ks):
-            steps = []
-            for p in range(PIECES):
-                steps.append(lambda p=p: [forward_strip(k, p) for k in ks])
-            steps.append(lambda: [forward_share(k) for k in ks])
-            return steps
-
-        for load in loads[:2]:
-            load.wait()
-        waiting = arrivals(phases[0])
-        expert_own(0)
-        waiting.pop(0)()
-        loads[2].wait()
-        expert_pair(0)
-        waiting.pop(0)()
-        down_own(0)
-        take_pair([0])
-        finish([0], 0, CHUNKS)
-        for index, ks in enumerate(phases):
-            while waiting:
-                waiting.pop(0)()
-            waiting = arrivals(phases[index + 1]) if index + 1 < len(phases) else []
-            for p in range(PIECES):
-                for k in ks:
-                    forward_swap(k, p)
-                if waiting and p < 2:
-                    waiting.pop(0)()
-            for k in ks:
-                expert_own(k)
-            for k in ks:
-                down_own(k)
-            for k in ks:
-                expert_pair(k)
-                if waiting:
-                    waiting.pop(0)()
-            take_pair(ks)
-            if index + 1 == len(phases) and index:
-
-                def last(q, carry, ks=ks):
-                    for k in ks:
-                        settle(k, q)
-                    for k in phases[-2]:
-                        settle(k, q + LEAD)
-                    return carry
-
-                lax.fori_loop(0, CHUNKS - LEAD, last, 0)
-                finish(ks, CHUNKS - LEAD, CHUNKS)
-            else:
-                finish(ks, 0, LEAD if index + 2 == len(phases) else CHUNKS)
-
-        def z_copy(q, step):
-            dst = place.z_peer(step)
+        for copy in loads:
+            copy.wait()
+        for copy in traded:
+            copy.wait_recv()
+        head = len(phases[0])
+        for k, p in near[:head]:
+            forward_strip(k, p)
+        serve(0)
+        for k, p in near[head:]:
+            forward_strip(k, p)
+        for k, p in near:
+            swaps[k, p].wait_recv()
+        for k, i in halves:
+            shares[k, i].wait_recv()
+        rest = [k for ks in phases for k in ks if k not in final]
+        coming = list(far)
+        for k in rest:
+            if coming:
+                forward_strip(*coming.pop(0))
+            serve(k)
+            reply([k], 0, LEAD)
+        while coming:
+            forward_strip(*coming.pop(0))
+        for k, p in far:
+            swaps[k, p].wait_recv()
+        for k in final:
+            serve(k)
+
+        def rest_of(q, carry):
+            for k in final:
+                back_copy(k, q).start()
+            for k in rest:
+                back_copy(k, q + LEAD).start()
+            return carry
+
+        lax.fori_loop(0, CHUNKS - LEAD, rest_of, 0)
+        reply(final, CHUNKS - LEAD, CHUNKS)
+
+        levels = n_z.bit_length() - 1
+
+        def z_blocks(level):
+            span = 2 << level
+            keep = lax.rem(z, span)
+            base = n_z - (n_z >> level)
+            return [
+                (j * span + keep, j * span + flip(keep, 1 << level), base + j)
+                for j in range(n_z // span)
+            ]
+
+        def z_copy(q, level, sent_block, slot):
             return remote(
-                cbuf.at[dst, :, column(q)], fbuf.at[z, :, column(q)],
-                sent.at[6], z_r.at[q, step], place.z_id(dst),
-            )
-
-        def combine(q, carry):
+                cbuf.at[sent_block, :, column(q)], fbuf.at[slot, :, column(q)],
+                sent.at[4], z_r.at[q, slot], place.z_id(flip(z, 1 << level)),
+            )
+
+        def combine(q):
             for k in range(1, n_sp):
                 back_copy(k, q).wait_recv()
             total = None
@@ -291,31 +270,48 @@
                 more = split_dot(mix_in[src], rbuf[src, :, column(q)], TN)
                 total = more if total is None else total + more
             cbuf[:, :, column(q)] = total.astype(jnp.bfloat16).reshape(n_z, tok, width)
-            for step in range(1, n_z):
-                z_copy(q, step).start()
+            for _, sent_block, slot in z_blocks(0):
+                z_copy(q, 0, sent_block, slot).start()
+
+        def add_level(q, level):
+            for kept, sent_block, slot in z_blocks(level):
+                z_copy(q, level, sent_block, slot).wait_recv()
+                total = cbuf[kept, :, column(q)].astype(jnp.float32) + fbuf[
+                    slot, :, column(q)
+                ].astype(jnp.float32)
+                if level + 1 == levels:
+                    o_ref[:, column(q)] = (total + mid_in[:, column(q)]).astype(jnp.bfloat16)
+                else:
+                    cbuf[kept, :, column(q)] = total.astype(jnp.bfloat16)
+            if level + 1 < levels:
+                for _, sent_block, slot in z_blocks(level + 1):
+                    z_copy(q, level + 1, sent_block, slot).start()
+
+        def wave(i, carry):
+            for stage in range(levels + 1):
+                q = i - LAG * stage
+
+                @pl.when((q >= 0) & (q < CHUNKS))
+                def _(q=q, stage=stage):
+                    if stage == 0:
+                        combine(q)
+                    else:
+                        add_level(q, stage - 1)
+
             return carry
 
-        lax.fori_loop(0, CHUNKS, combine, 0)
-
-        def close(q, carry):
-            total = mid_in[:, column(q)] + cbuf[z, :, column(q)].astype(jnp.float32)
-            for step in range(1, n_z):
-                z_copy(q, step).wait_recv()
-                total += fbuf[lax.rem(z - step + n_z, n_z), :, column(q)].astype(jnp.float32)
-            o_ref[:, column(q)] = total.astype(jnp.bfloat16)
-            return carry
-
-        lax.fori_loop(0, CHUNKS, close, 0)
-
-        others = pl.ds(0, n_sp - 1)
-        strip_bytes = xbuf.at[0, others, :, pl.ds(shared, half)]
+        lax.fori_loop(0, CHUNKS, wave, 0)
+        lax.fori_loop(CHUNKS, CHUNKS + LAG * levels, wave, 0)
+        strip_bytes = xbuf.at[:, :, pl.ds(0, quarter)]
         for kind, block in enumerate(
             (
-                strip_bytes, xbuf.at[0, others, :, both], strip_bytes, ybuf, ybuf,
-                ybuf.at[others], fbuf.at[pl.ds(0, n_z - 1)],
+                strip_bytes, xbuf.at[pl.ds(0, n_sp - 2), :, pl.ds(0, 2 * quarter)],
+                strip_bytes, sbuf.at[pl.ds(0, n_sp - 1)], fbuf.at[pl.ds(0, n_z - 1)],
             )
         ):
-            remote(block, block, sent.at[kind], z_r.at[0, 0], partner).wait_send()
+            remote(block, block, sent.at[kind], z_r.at[0, 0], place.partner()).wait_send()
+        for copy in traded:
+            copy.wait_send()
 
     dma = pltpu.SemaphoreType.DMA
     bf = jnp.bfloat16
@@ -324,21 +320,20 @@
     return dict(
         body=body,
         loads=loads_of,
+        shares=shares_of,
         ins=(gate, up, down),
         scratch=[
-            pltpu.VMEM(gate.shape, bf),
-            pltpu.VMEM(up.shape, bf),
-            pltpu.VMEM(down.shape, bf),
-            pltpu.VMEM((2, n_sp, rows, D), bf),
-            pltpu.VMEM((2, n_sp, rows, hidden), bf),
-            block, block, block, block, zblock, zblock,
-            dma((3,)),
-            dma((7,)),
+            pltpu.VMEM((D, 2 * hidden), bf),
+            pltpu.VMEM((D, 2 * hidden), bf),
+            pltpu.VMEM((2 * hidden, D), bf),
+            block,
+            pltpu.VMEM((1, rows, 2 * hidden), bf),
+            block, block, zblock, zblock,
+            dma((9,)),
+            dma((5,)),
             dma((n_sp, PIECES)),
-            dma((n_sp,)),
+            dma((n_sp, 2)),
             dma((n_sp, PIECES)),
-            dma((n_sp,)),
-            dma((n_sp,)),
             dma((n_sp, CHUNKS)),
             dma((CHUNKS, n_z)),
         ],
@@ -369,7 +364,11 @@
         place = Place(n_sp, n_z)
         ins, weights, refs = refs[:n_ins], refs[n_ins : n_ins + 3], refs[n_ins + 3 :]
         o_ref, held, refs = refs[0], refs[1 : 1 + n_given], refs[1 + n_given :]
-        drain = first["body"](place, ins, held, refs[:n_first], second["loads"](weights, refs[n_first:]))
+        later = refs[n_first:]
+        drain = first["body"](
+            place, ins, held, refs[:n_first], second["loads"](place, weights, later),
+            second["shares"](place, weights, later),
+        )
         second["body"](place, held, weights, o_ref, refs[n_first:])
         drain()
 
@@ -387,14 +386,16 @@
     def head(*refs):
         place = Place(n_sp, n_z)
         ins, outs = refs[:n_ins], refs[n_ins : n_ins + n_given]
-        first["body"](place, ins, outs, refs[n_ins + n_given :], [])()
+        first["body"](place, ins, outs, refs[n_ins + n_given :], [], [])()
 
     def tail(*refs):
         place = Place(n_sp, n_z)
         scratch = refs[n_given + 4 :]
-        for load in second["loads"](refs[n_given : n_given + 3], scratch):
+        for load in second["loads"](place, refs[n_given : n_given + 3], scratch):
             load.start()
         place.barrier(True, True)
+        for copy in second["shares"](place, refs[n_given : n_given + 3], scratch):
+            copy.start()
         second["body"](
             place, refs[:n_given], refs[n_given : n_given + 3], refs[n_given + 3], scratch
         )
@@ -452,7 +453,7 @@
     freqs = ROPE // 2
     inverse = np.float32(rope_base) ** (-np.arange(0, ROPE, 2, dtype=np.float32) / np.float32(ROPE))
 
-    def body(place, ins, outs, scratch, more_loads):
+    def body(place, ins, outs, scratch, more_loads, more_sends):
         (
             q_hbm, lat_hbm, rot_in, latg, kup_hbm, vup_hbm, qg, kg, outg, w_hbm, res_hbm, ffng,
             routes_in, weights_in,
@@ -545,6 +546,9 @@
         (q_nope_gain, q_rot_gain), (k_nope_gain, k_rot_gain) = packed
 
         pl.semaphore_wait(sem, n_tp - 1 + n_sp - 1)
+        for copy in more_sends:
+            copy.start()
+
         def push(src, dst, kind, recv, device):
             copy = remote(src, dst, sent.at[kind], recv, device)
             copy.start()
@@ -723,7 +727,7 @@
                 acc[at, :] = new if first else acc[at, :] * fade + new
                 return carry
 
-            lax.fori_loop(0, length // qt, tile, 0)
+            lax.fori_loop(0, length // qt, tile, 0, unroll=2)
 
         attend(sp, True, True)
 
@@ -758,9 +762,24 @@
             att[block % 2, (block // 2) * tok : (block // 2 + 1) * tok, :] = (
                 acc[at, :] / bottom
             ).astype(jnp.bfloat16)
-        for step in range(n_tp - 1, 0, -1):
-            dst = lax.rem(tp + step, n_tp)
-            push(att.at[lax.rem(dst, 2)], gath.at[tp], 2, att_r.at[tp], (sp, dst))
+        def att_copy(src, parity, to_z, to_core, src_ref=None):
+            block = gath.at[src]
+            from_ref = block if src_ref is None else src_ref.at[parity]
+            return remote(
+                from_ref, block, sent.at[2], att_r.at[src], (sp, 2 * to_z + to_core)
+            )
+
+        for away in (2, -2, 1, -1):
+            to = z + away
+
+            @pl.when((to >= 0) & (to < n_z))
+            def _(to=to):
+                for parity in range(2):
+                    att_copy(tp, parity, to, parity, att).start()
+
+        remote(
+            att.at[1 - core], gath.at[tp], sent.at[2], att_r.at[tp], place.partner()
+        ).start()
         own = pltpu.make_async_copy(att.at[core], gath.at[tp], load_sem.at[6])
         own.start()
 
@@ -793,10 +812,24 @@
         for load in loads[4:]:
             load.wait()
         own.wait()
-        for step in range(1, n_tp):
-            src = lax.rem(tp + step, n_tp)
-            block = gath.at[src]
-            remote(block, block, sent.at[2], att_r.at[src], partner).wait_recv()
+        for away in range(2, n_z - 1):
+            for sign in (1, -1):
+                src, to = z - sign * away, z + sign
+
+                @pl.when((src >= 0) & (src < n_z) & (to >= 0) & (to < n_z))
+                def _(src=src, to=to):
+                    for which in range(2):
+                        att_copy(2 * src + which, core, z, core).wait_recv()
+                        att_copy(2 * src + which, core, to, core).start()
+
+        for src in range(n_tp):
+            away = z - src // 2
+            passed = ((away >= 2) & (z + 1 < n_z)) | ((away <= -2) & (z > 0))
+
+            @pl.when((tp != src) & jnp.logical_not(passed))
+            def _(src=src):
+                att_copy(src, core, z, core).wait_recv()
+
         square = None
         for t in range(n_tp):
             block = gath[t].astype(jnp.float32)
@@ -849,8 +882,24 @@
 
             block = metabuf.at[pl.ds(0, n_z - 1)]
             remote(block, block, sent.at[1], meta_r.at[0], partner).wait_send()
-            block = gath.at[pl.ds(0, n_tp - 1)]
-            remote(block, block, sent.at[2], att_r.at[0], partner).wait_send()
+            one = att_copy(tp, core, z, core)
+            one.wait_send()
+            for away in (2, -2, 1, -1):
+
+                @pl.when((z + away >= 0) & (z + away < n_z))
+                def _():
+                    one.wait_send()
+                    one.wait_send()
+
+            for away in range(2, n_z - 1):
+                for sign in (1, -1):
+                    src, to = z - sign * away, z + sign
+
+                    @pl.when((src >= 0) & (src < n_z) & (to >= 0) & (to < n_z))
+                    def _():
+                        one.wait_send()
+                        one.wait_send()
+
             for step in range(1, n_sp):
                 dst = sp + n_sp - step
 

time: 104 us -> 99.1 us (0.953)
  the two profiles are of different devices: /device:TPU:4 before, /device:TPU:0 now
where the time goes in v4:
time: 99.1 us; the launch traced here: 98.9 us
  Pallas kernels  97.3 us (98%)
  local copies, waits for them, and re-layouts  1.67 us (2%)
    pallas_call x1, Pallas kernels, run_plans(): pl.pallas_call(merged, out_shape=out_shape, in_specs=first['in_specs'] +...  97.3 us

profile of v4, /device:TPU:0, one launch (start us, length us, event | category | flops | bytes accessed | tf_op | source)
XLA Modules:
  0.0 98.9 jit_solution(13769131068395464492)
XLA Ops:
  0.0 97.3 %layer.1 = bf16[64,2048]{1,0:T(8,128)(2,1)} custom-call(bf16[192,512]{1,0:T(8,128)(2,1)} %bitcast.15, bf16[512,512]{1,0:T(8,128)(2,1)} %refs_1_.1, bf16[32,512]{1,0:T(8,128)(2,1)} %bitcast.16, f32[1,512]{1,0:T(1,128)} %bitcast.19, bf16[512,128]{1,0:T(8,128)(2,1)} %refs_4_.1, bf16[512,128]{1,0:T(8,128)(2,1)} %refs_5_.1, f32[1,96]{1,0:T(1,128)} %bitcast.22, ...), custom_call_target="tpu_custom_call" | custom-call | tf_op jit(solution)/shard_map/layer/pallas_call | solution.py:376
  97.3 1.7 %copy.19 = bf16[64,2048]{1,0:T(8,128)(2,1)} copy(bf16[64,2048]{1,0:T(8,128)(2,1)} %layer.1) | data formatting | bytes 524288

commit v5 on v4

--- a/solution.py
+++ b/solution.py
@@ -219,11 +219,12 @@
             forward_strip(k, p)
         for k, p in near:
             swaps[k, p].wait_recv()
-        for k, i in halves:
-            shares[k, i].wait_recv()
         rest = [k for ks in phases for k in ks if k not in final]
         coming = list(far)
+        forward_strip(*coming.pop(0))
         for k in rest:
+            for i in range(2):
+                shares[k, i].wait_recv()
             if coming:
                 forward_strip(*coming.pop(0))
             serve(k)

time: 99.1 us -> 97.5 us (0.984)
  Pallas kernels: 97.3 us -> 95.6 us
    pallas_call x1, Pallas kernels: 97.3 us -> 95.6 us  [run_plans(): pl.pallas_call(merged, out_shape=out_shape, in_specs=first['in_specs'] +...]
where the time goes in v5:
time: 97.5 us; the launch traced here: 97.3 us
  Pallas kernels  95.6 us (98%)
  local copies, waits for them, and re-layouts  1.67 us (2%)
    pallas_call x1, Pallas kernels, run_plans(): pl.pallas_call(merged, out_shape=out_shape, in_specs=first['in_specs'] +...  95.6 us

profile of v5, /device:TPU:0, one launch (start us, length us, event | category | flops | bytes accessed | tf_op | source)
XLA Modules:
  0.0 97.3 jit_solution(7811729340944050782)
XLA Ops:
  0.0 95.6 %layer.1 = bf16[64,2048]{1,0:T(8,128)(2,1)} custom-call(bf16[192,512]{1,0:T(8,128)(2,1)} %bitcast.15, bf16[512,512]{1,0:T(8,128)(2,1)} %refs_1_.1, bf16[32,512]{1,0:T(8,128)(2,1)} %bitcast.16, f32[1,512]{1,0:T(1,128)} %bitcast.19, bf16[512,128]{1,0:T(8,128)(2,1)} %refs_4_.1, bf16[512,128]{1,0:T(8,128)(2,1)} %refs_5_.1, f32[1,96]{1,0:T(1,128)} %bitcast.22, ...), custom_call_target="tpu_custom_call" | custom-call | tf_op jit(solution)/shard_map/layer/pallas_call | solution.py:377
  95.6 1.7 %copy.19 = bf16[64,2048]{1,0:T(8,128)(2,1)} copy(bf16[64,2048]{1,0:T(8,128)(2,1)} %layer.1) | data formatting | bytes 524288

commit v6 on v5

--- a/solution.py
+++ b/solution.py
@@ -87,7 +87,7 @@
 CHUNKS = 8
 PIECES = 4
 WIDE = 512
-LEAD = 5
+LEAD = 3
 LAG = 2
 
 
@@ -157,14 +157,16 @@
         far = [one for one in order if one[0] in final]
         for k, p in near:
             push_strip(k, p)
-        for k, i in halves:
-            dst = flip(me, k)
-            shares[k, i] = push(
-                x_in.at[dst, :, both[i]], xbuf.at[me, :, both[i]], 1, b_r.at[k, i],
-                place.sp_id(dst),
-            )
-        for k, p in far:
-            push_strip(k, p)
+        for i in range(2):
+            for k, which in halves:
+                if which == i:
+                    dst = flip(me, k)
+                    shares[k, i] = push(
+                        x_in.at[dst, :, both[i]], xbuf.at[me, :, both[i]], 1, b_r.at[k, i],
+                        place.sp_id(dst),
+                    )
+            for k, p in far[i * PIECES // 2 : (i + 1) * PIECES // 2]:
+                push_strip(k, p)
 
         def forward_strip(k, p):
             block = xbuf.at[flip(me, k), :, strip(side, k, p)]
@@ -221,14 +223,15 @@
             swaps[k, p].wait_recv()
         rest = [k for ks in phases for k in ks if k not in final]
         coming = list(far)
-        forward_strip(*coming.pop(0))
+        for _ in range(PIECES // 2 if coming else 0):
+            forward_strip(*coming.pop(0))
         for k in rest:
             for i in range(2):
                 shares[k, i].wait_recv()
+            serve(k)
+            reply([k], 0, LEAD)
             if coming:
                 forward_strip(*coming.pop(0))
-            serve(k)
-            reply([k], 0, LEAD)
         while coming:
             forward_strip(*coming.pop(0))
         for k, p in far:

time: 97.5 us -> 96.8 us (level)
  no operation moved by 1% of the time
where the time goes in v6:
time: 96.8 us; the launch traced here: 96.6 us
  Pallas kernels  94.9 us (98%)
  local copies, waits for them, and re-layouts  1.67 us (2%)
    pallas_call x1, Pallas kernels, run_plans(): pl.pallas_call(merged, out_shape=out_shape, in_specs=first['in_specs'] +...  94.9 us

profile of v6, /device:TPU:0, one launch (start us, length us, event | category | flops | bytes accessed | tf_op | source)
XLA Modules:
  0.0 96.6 jit_solution(6391772589930005659)
XLA Ops:
  0.0 94.9 %layer.1 = bf16[64,2048]{1,0:T(8,128)(2,1)} custom-call(bf16[192,512]{1,0:T(8,128)(2,1)} %bitcast.15, bf16[512,512]{1,0:T(8,128)(2,1)} %refs_1_.1, bf16[32,512]{1,0:T(8,128)(2,1)} %bitcast.16, f32[1,512]{1,0:T(1,128)} %bitcast.19, bf16[512,128]{1,0:T(8,128)(2,1)} %refs_4_.1, bf16[512,128]{1,0:T(8,128)(2,1)} %refs_5_.1, f32[1,96]{1,0:T(1,128)} %bitcast.22, ...), custom_call_target="tpu_custom_call" | custom-call | tf_op jit(solution)/shard_map/layer/pallas_call | solution.py:380
  94.9 1.7 %copy.19 = bf16[64,2048]{1,0:T(8,128)(2,1)} copy(bf16[64,2048]{1,0:T(8,128)(2,1)} %layer.1) | data formatting | bytes 524288
